TPU v7x, 32 devices: a whole 2x2x4 slice. The times are simulated.
32 devices in a mesh: grp: 2 (over x), row: 4 (over z), col: 4 (over y, core).
Axes of the slice: x: 2, y: 2, z: 4, core: 2. Of those that a mesh axis runs over, the one named last changes fastest.
Arguments:
- gate_in: bfloat16 [8, 512, 1024], P(('grp', 'row'), 'col'), parts along dimension 0, may hold values from -6 to 6
- mult_in: bfloat16 [8, 512, 1024], P(('grp', 'row'), 'col'), parts along dimension 0, may hold values from -6 to 6
- value_in: bfloat16 [8, 512, 1024], P(('grp', 'row'), 'col'), parts along dimension 0, may hold values from -6 to 6
- taps_gate: float32 [3, 1024], replicated, may hold values from -3.5 to 3.5
- taps_mult: float32 [3, 1024], replicated, may hold values from -3.5 to 3.5
- taps_value: float32 [3, 1024], replicated, may hold values from -3.5 to 3.5
- filter_first: float32 [33, 128], replicated, may hold values from -3 to 3
- filter_second: float32 [128, 128], replicated, may hold values from -1 to 1
- filter_ahead: float32 [128, 1024], replicated, may hold values from -0.5 to 0.5
- filter_behind: float32 [128, 1024], replicated, may hold values from -0.5 to 0.5
- filter_decay: float32 [1024], replicated, may hold values from 0.05 to 17.033333
- skip_gain: float32 [1024], replicated, may hold values from -5 to 5
- out_weight: bfloat16 [1024, 2048], replicated, may hold values from -0.1875 to 0.1875
Outputs:
- mixed: bfloat16 [8, 512, 2048], P(('grp', 'row'), 'col'), parts along dimension 0
There are 2 independent parts, one for each index of `grp`. A program takes and returns all parts, laid end to end along the dimension named above; an argument that names none is the same for every part. Nothing has to cross between parts.
All inputs are finite; a program needn't handle non-finite values.
Results may differ from a plain program's by a relative error of at most 0.0049.
Values may be sent and summed in bfloat16 or wider, within the bound.
A program may use at most 64 MiB of HBM per device.

v0:
```python
import functools
import math

import jax
import jax.numpy as jnp
import numpy as np
from jax import lax
from jax.experimental import pallas as pl
from jax.experimental.pallas import tpu as pltpu
from jax.sharding import PartitionSpec as P

highest = lax.Precision.HIGHEST


def padded_2(shard, sides, width):
    for axis, dim in sides:
        size, length = (lax.axis_size(axis), shard.shape[dim])
        up = [(i, (i + 1) % size) for i in range(size - 1)]
        down = [(j, i) for i, j in up]
        last = lax.slice_in_dim(shard, length - width, length, axis=dim)
        leading = lax.slice_in_dim(shard, 0, width, axis=dim)
        before = lax.ppermute(last, axis, up)
        after = lax.ppermute(leading, axis, down)
        shard = jnp.concatenate([before, shard, after], axis=dim)
    return shard


def filter_hidden(mirror, seq_len, filter_first, filter_second):
    tau_values = mirror.astype(jnp.float32) / (seq_len - 1)
    omega_pos = 2.0 * math.pi / seq_len * mirror.astype(jnp.float32)
    band_count = (filter_first.shape[0] - 1) // 2
    band_values = jnp.linspace(0.0001, band_count - 1, band_count, dtype=jnp.float32)
    angles = omega_pos[:, None] * band_values[None, :]
    features = jnp.concatenate([tau_values[:, None], jnp.cos(angles), -jnp.sin(angles)], axis=1)
    hidden = jnp.sin(jnp.dot(features, filter_first, precision=highest))
    hidden = jnp.sin(jnp.dot(hidden, filter_second, precision=highest))
    return (hidden, tau_values)


def side_values(hidden, tau_values, side_weight, decay_rates):
    values = jnp.einsum("pf,fh->hp", hidden, side_weight, precision=highest)
    return values * jnp.exp(-decay_rates[:, None] * tau_values[None, :])


def angle_table(row_count, column_count, period):
    products = (
        lax.iota(jnp.int32, row_count)[:, None]
        * lax.iota(jnp.int32, column_count)[None, :]
        % period
    )
    angle = products.astype(jnp.float32) * (2.0 * math.pi / period)
    return (jnp.cos(angle), jnp.sin(angle))


def swap_halves(stacked, width):
    return jnp.concatenate([stacked[..., width:], stacked[..., :width]], axis=-1)


def forward(values, first_table, twist_even, twist_odd, second_block):
    channels, _, width = values.shape
    first = jnp.einsum("sfa,cab->cfsb", first_table, values, precision=highest)
    first = first.reshape(channels, first_table.shape[1], 2 * width)
    turned = first * twist_even + swap_halves(first, width) * twist_odd
    return jnp.einsum("cfk,kl->cfl", turned, second_block, precision=highest)


def inverse(spectrum, last_table, twist_even, twist_odd, second_block, span_len):
    channels, freq_rows, double_width = spectrum.shape
    width = double_width // 2
    back = jnp.einsum("cfk,kl->cfl", spectrum, second_block, precision=highest)
    turned = back * twist_even + swap_halves(back, width) * twist_odd
    turned = turned.reshape(channels, freq_rows, 2, width)
    result = jnp.einsum("asf,cfsb->cab", last_table, turned, precision=highest)
    return result / span_len


def spread_body(
    gate_in,
    mult_in,
    value_in,
    taps_gate,
    taps_mult,
    taps_value,
    filter_first,
    filter_second,
    filter_ahead,
    filter_behind,
    filter_decay,
    skip_gain,
    out_weight,
):
    col_count = lax.axis_size("col")
    col_index = lax.axis_index("col")
    tok_rows = gate_in.shape[1]
    seq_len = tok_rows * col_count
    span_len = 2 * seq_len
    group_size = filter_ahead.shape[1] // col_count
    stacked = jnp.stack([gate_in[0], mult_in[0], value_in[0]])
    padded = padded_2(stacked, (("col", 1),), 1).astype(jnp.float32)
    all_taps = jnp.stack([taps_gate, taps_mult, taps_value])
    shorted = jnp.zeros(stacked.shape, jnp.float32)
    for offset in range(all_taps.shape[1]):
        shorted = shorted + all_taps[:, offset][:, None, :] * padded[:, offset : offset + tok_rows]
    gate_part = shorted[0]
    product = shorted[2] * shorted[1]
    spread = lax.all_to_all(product.T, "col", split_axis=0, concat_axis=1, tiled=True)
    first_channel = col_index * group_size
    own_rates = lax.dynamic_slice_in_dim(filter_decay, first_channel, group_size)
    mirror = lax.iota(jnp.int32, seq_len)
    hidden, tau_values = filter_hidden(mirror, seq_len, filter_first, filter_second)
    ahead_vals = side_values(
        hidden,
        tau_values,
        lax.dynamic_slice_in_dim(filter_ahead, first_channel, group_size, 1),
        own_rates,
    )
    behind_vals = side_values(
        hidden,
        tau_values,
        lax.dynamic_slice_in_dim(filter_behind, first_channel, group_size, 1),
        own_rates,
    )
    kernel = jnp.concatenate(
        [ahead_vals, jnp.zeros((group_size, 1), jnp.float32), jnp.flip(behind_vals[:, 1:], axis=1)],
        axis=1,
    )
    kernel = kernel * lax.rsqrt(jnp.sum(kernel * kernel, axis=1, keepdims=True) + 1e-06)
    factor = 128
    half_rows = factor // 2
    width_second = span_len // factor
    first_cos, first_sin = angle_table(factor, factor, factor)
    twist_cos, twist_sin = angle_table(factor, width_second, span_len)
    second_cos, second_sin = angle_table(width_second, width_second, width_second)
    first_table = jnp.stack([first_cos, -first_sin])
    last_table = jnp.stack([first_cos[:half_rows], -first_sin[:half_rows]], axis=1)
    twist_even = jnp.concatenate([twist_cos, twist_cos], axis=1)
    twist_ahead = jnp.concatenate([twist_sin, -twist_sin], axis=1)
    twist_back = jnp.concatenate([-twist_sin, twist_sin], axis=1)
    block_ahead = jnp.concatenate(
        [
            jnp.concatenate([second_cos, -second_sin], axis=1),
            jnp.concatenate([second_sin, second_cos], axis=1),
        ],
        axis=0,
    )
    block_back = jnp.concatenate(
        [
            jnp.concatenate([second_cos, second_sin], axis=1),
            jnp.concatenate([-second_sin, second_cos], axis=1),
        ],
        axis=0,
    )
    kernel_spec = forward(
        kernel.reshape(group_size, factor, width_second),
        first_table,
        twist_even,
        twist_ahead,
        block_ahead,
    )
    data_spec = forward(
        spread.reshape(group_size, half_rows, width_second),
        first_table[:, :, :half_rows],
        twist_even,
        twist_ahead,
        block_ahead,
    )
    data_re = data_spec[..., :width_second]
    data_im = data_spec[..., width_second:]
    kernel_re = kernel_spec[..., :width_second]
    kernel_im = kernel_spec[..., width_second:]
    joined = jnp.concatenate(
        [data_re * kernel_re - data_im * kernel_im, data_re * kernel_im + data_im * kernel_re],
        axis=-1,
    )
    convolved = inverse(joined, last_table, twist_even, twist_back, block_back, span_len).reshape(
        group_size, seq_len
    )
    returned = lax.all_to_all(convolved, "col", split_axis=1, concat_axis=0, tiled=True)
    mixed_rows = ((returned.T + skip_gain * product) * gate_part).astype(jnp.bfloat16)
    return jnp.dot(mixed_rows, out_weight, preferred_element_type=jnp.float32).astype(jnp.bfloat16)[
        None
    ]


f32, bf16 = (jnp.float32, jnp.bfloat16)
EDGE = 16
PARTS = 2


def wave_tables(seq_len):
    odd = 2 * np.arange(seq_len, dtype=np.int64) + 1
    angle = (odd[:, None] * odd[None, :] % (8 * seq_len)) * (math.pi / (4 * seq_len))
    pieces = []
    for table in (np.cos(angle), np.sin(angle)):
        high = table.astype(bf16)
        pieces += [high, (table - high.astype(np.float64)).astype(bf16)]
    half = odd * (math.pi / (4 * seq_len))
    turn = np.stack([np.cos(half), np.sin(half)]).astype(np.float32)
    turn = np.repeat(turn[:, :, None], 128, axis=2)
    return (np.stack(pieces), turn)


def feature_table(seq_len, feature_count):
    position = np.arange(seq_len, dtype=np.float64)
    bands = (feature_count - 1) // 2
    values = np.linspace(0.0001, bands - 1, bands)
    angles = (2.0 * math.pi / seq_len * position)[:, None] * values[None, :]
    tau = position / (seq_len - 1)
    table = np.concatenate([tau[:, None], np.cos(angles), -np.sin(angles)], axis=1)
    return np.pad(table, ((0, 0), (0, 128 - feature_count))).astype(np.float32)


def sine(x):
    turns = jnp.floor(x * (1.0 / math.pi) + 0.5)
    r = x - turns * 3.140625
    r = r - turns * 9.67502593994140625e-4
    r = r - turns * 1.509957990978376432e-7
    sign = 1.0 - 2.0 * (turns - 2.0 * jnp.floor(turns * 0.5))
    s = r * r
    poly = 1.0 / 362880.0 - s * (1.0 / 39916800.0)
    poly = -1.0 / 5040.0 + s * poly
    poly = 1.0 / 120.0 + s * poly
    poly = -1.0 / 6.0 + s * poly
    return sign * (r + r * s * poly)


def split(value):
    high = value.astype(bf16)
    return (high, (value - high.astype(f32)).astype(bf16))


def mul(a, b):
    return jnp.dot(a, b, preferred_element_type=f32)


def mul_precise(a, b):
    return jnp.dot(a, b, preferred_element_type=f32, precision=highest)


def neighbours(rows, before, after):
    count = rows.shape[0]
    index = lax.broadcasted_iota(jnp.int32, rows.shape, 0)
    up = jnp.where(index == 0, before, pltpu.roll(rows, 1, 0))
    down = jnp.where(index == count - 1, after, pltpu.roll(rows, count - 1, 0))
    return (up, down)


def short_form(rows, taps, before, after):
    up, down = neighbours(rows, before, after)
    return taps[0:1] * up + taps[1:2] * rows + taps[2:3] * down


def conv_kernel(
    n,
    gate_hbm,
    mult_hbm,
    value_hbm,
    taps_gate_hbm,
    taps_mult_hbm,
    taps_value_hbm,
    first_hbm,
    second_hbm,
    ahead_hbm,
    behind_hbm,
    decay_hbm,
    skip_hbm,
    weight_hbm,
    table_hbm,
    turn_hbm,
    feature_hbm,
    out_ref,
    gate,
    mult,
    value,
    taps_gate,
    taps_mult,
    taps_value,
    second_ref,
    decay_ref,
    skip_ref,
    first,
    ahead_w,
    behind_w,
    weight,
    table,
    turn,
    feature,
    sent,
    came,
    whole,
    back_sent,
    back_came,
    halo_sent,
    halo_came,
    kernel_re,
    kernel_im,
    spec,
    gate_part,
    direct,
    total,
    load_sems,
    send_sems,
    recv_sems,
    back_send,
    back_recv,
    halo_send,
    halo_recv,
):
    me = lax.axis_index("col")
    rows, channels = gate.shape
    group = channels // n
    seq_len = rows * n
    near = me + 1 - 2 * lax.rem(me, 2)
    peers = []
    for j in range(1, n // 2):
        peers += [lax.rem(me + 2 * j, n), lax.rem(near + 2 * j, n)]
    peers.append(near)

    def columns(owner):
        return pl.ds(pl.multiple_of(owner * group, group), group)

    loads = [
        pltpu.make_async_copy(s, d, load_sems.at[i])
        for i, (s, d) in enumerate(
            [
                (value_hbm.at[0], value),
                (mult_hbm.at[0], mult),
                (taps_value_hbm, taps_value),
                (taps_mult_hbm, taps_mult),
                (feature_hbm, feature),
                (first_hbm, first.at[pl.ds(0, first_hbm.shape[0])]),
                (second_hbm, second_ref),
                (decay_hbm, decay_ref),
                (ahead_hbm.at[:, columns(me)], ahead_w),
                (behind_hbm.at[:, columns(me)], behind_w),
                (table_hbm, table),
                (turn_hbm, turn),
                (gate_hbm.at[0], gate),
                (taps_gate_hbm, taps_gate),
                (skip_hbm, skip_ref),
                (weight_hbm, weight),
            ]
        )
    ]
    for load in loads:
        load.start()
    barrier = pltpu.get_barrier_semaphore()
    for peer in peers:
        pl.semaphore_signal(
            barrier, inc=1, device_id={"col": peer}, device_id_type=pl.DeviceIdType.MESH
        )
    for load in loads[:4]:
        load.wait()

    part = group // PARTS

    def piece(owner, h):
        return pl.ds(pl.multiple_of(owner * group + h * part, part), part)

    def pack(owner, h):
        cols = piece(owner, h)
        v = value[:, cols].astype(f32)
        m = mult[:, cols].astype(f32)
        zero = jnp.zeros((1, part), f32)
        vs = short_form(v, taps_value[:, cols], zero, zero)
        ms = short_form(m, taps_mult[:, cols], zero, zero)
        sent[h, owner, pl.ds(0, rows), :] = (vs * ms).astype(bf16)
        edges = jnp.concatenate(
            [v[0:2], v[rows - 2 : rows], m[0:2], m[rows - 2 : rows], jnp.zeros((8, part), f32)], axis=0
        )
        sent[h, owner, pl.ds(rows, EDGE), :] = edges.astype(bf16)

    def remote(src, dst, ssem, rsem, peer):
        return pltpu.make_async_remote_copy(
            src_ref=src,
            dst_ref=dst,
            send_sem=ssem,
            recv_sem=rsem,
            device_id={"col": peer},
            device_id_type=pl.DeviceIdType.MESH,
        )

    copies = []
    for h in range(PARTS):
        for i, peer in enumerate(peers):
            pack(peer, h)
            if i + h == 0:
                pl.semaphore_wait(barrier, n - 1)
            copy = remote(
                sent.at[h, peer], came.at[h, me], send_sems.at[h, peer], recv_sems.at[h, me], peer
            )
            copy.start()
            copies.append(copy)
    loads[12].wait()
    right, left = (lax.rem(me + 1, n), lax.rem(me + n - 1, n))
    for side, (row, target) in enumerate([(rows - 1, right), (0, left)]):
        base = rows - EDGE if row else 0
        at = row - base
        parts = [r[base : base + EDGE, :].astype(f32)[at : at + 1] for r in (gate, mult, value)]
        tile = jnp.concatenate(parts + [jnp.zeros((EDGE - 3, channels), f32)], axis=0)
        halo_sent[side] = tile.astype(bf16)
        copy = remote(
            halo_sent.at[side], halo_came.at[side], halo_send.at[side], halo_recv.at[side], target
        )
        copy.start()
        copies.append(copy)
    for h in range(PARTS):
        pack(me, h)

    for load in loads[4:10]:
        load.wait()
    used = first_hbm.shape[0]
    at = lax.broadcasted_iota(jnp.int32, first.shape, 0)
    first_w = jnp.where(at < used, first[...], 0.0)
    hidden = sine(mul_precise(feature[...], first_w))
    hidden = sine(mul_precise(hidden, second_ref[...]))
    later = pltpu.roll(hidden, seq_len - 1, 0)
    rates = decay_ref[:, columns(me)]
    index = lax.broadcasted_iota(jnp.int32, (seq_len, group), 0)
    tau = index.astype(f32) * (1.0 / (seq_len - 1))
    fade = jnp.exp(-rates * tau)
    step = jnp.exp(-rates * (1.0 / (seq_len - 1)))
    ahead = mul_precise(hidden, ahead_w[...]) * fade
    behind = mul_precise(later, behind_w[...]) * (fade * step)
    behind = jnp.where(index == seq_len - 1, 0.0, behind)
    power = jnp.sum(ahead * ahead + behind * behind, axis=0, keepdims=True)
    scale = lax.rsqrt(power + 1e-06) * (2.0 / (2 * seq_len))
    loads[10].wait()
    loads[11].wait()
    high, low = split((ahead + behind) * scale)
    even = mul(table[0], high) + mul(table[1], high) + mul(table[0], low)
    high, low = split((ahead - behind) * scale)
    odd = mul(table[2], high) + mul(table[3], high) + mul(table[2], low)
    cos_half = turn[0][:, 0:1]
    sin_half = turn[1][:, 0:1]
    kernel_re[...] = cos_half * even + sin_half * odd
    kernel_im[...] = sin_half * even - cos_half * odd


    def near_product(h):
        whole[h, pl.ds(pl.multiple_of(me * rows, rows), rows), :] = sent[h, me, pl.ds(0, rows), :]
        came[h, me, pl.ds(rows, EDGE), :] = sent[h, me, pl.ds(rows, EDGE), :]
        for peer in reversed(peers):
            remote(
                sent.at[h, peer], came.at[h, peer], send_sems.at[h, peer], recv_sems.at[h, peer], peer
            ).wait_recv()
            whole[h, pl.ds(pl.multiple_of(peer * rows, rows), rows), :] = came[
                h, peer, pl.ds(0, rows), :
            ]
        edges = [came[h, s, pl.ds(rows, EDGE), :].astype(f32) for s in range(n)]
        own_taps = [t[:, piece(me, h)] for t in (taps_value, taps_mult)]
        tile_at = lax.broadcasted_iota(jnp.int32, (EDGE, part), 0)
        for s in range(n):
            top = bottom = 1.0
            for k, taps in enumerate(own_taps):
                e = edges[s][4 * k : 4 * k + 4]
                first_row = taps[1:2] * e[0:1] + taps[2:3] * e[1:2]
                last_row = taps[0:1] * e[2:3] + taps[1:2] * e[3:4]
                if s > 0:
                    first_row += taps[0:1] * edges[s - 1][4 * k + 3 : 4 * k + 4]
                if s < n - 1:
                    last_row += taps[2:3] * edges[s + 1][4 * k : 4 * k + 1]
                top, bottom = (top * first_row, bottom * last_row)
            for base, at, row in ((s * rows, 0, top), ((s + 1) * rows - EDGE, EDGE - 1, bottom)):
                old = whole[h, base : base + EDGE, :].astype(f32)
                whole[h, base : base + EDGE, :] = jnp.where(tile_at == at, row, old).astype(bf16)

    def invert(owner, h):
        take = pl.ds(pl.multiple_of(owner * rows, rows), rows)
        ch, cl, sh, sl = (table[i, take, :] for i in range(4))
        return (
            mul(ch, spec[h, 0]) + mul(sh, spec[h, 2])
            + mul(cl, spec[h, 0]) + mul(sl, spec[h, 2])
            + mul(ch, spec[h, 1]) + mul(sh, spec[h, 3])
        )

    for h in range(PARTS):
        near_product(h)
        x = whole[h]
        xc = mul(table[0], x) + mul(table[1], x)
        xs = mul(table[2], x) + mul(table[3], x)
        cols = slice(h * part, (h + 1) * part)
        kr, ki = (kernel_re[:, cols], kernel_im[:, cols])
        spec[h, 0], spec[h, 1] = split(xc * kr + xs * ki)
        spec[h, 2], spec[h, 3] = split(xs * kr - xc * ki)
        for peer in peers:
            back_sent[h, peer] = invert(peer, h).astype(bf16)
            copy = remote(
                back_sent.at[h, peer],
                back_came.at[h, me],
                back_send.at[h, peer],
                back_recv.at[h, me],
                peer,
            )
            copy.start()
            copies.append(copy)
    own_back = jnp.concatenate([invert(me, h) for h in range(PARTS)], axis=1)

    for side, target in enumerate((left, right)):
        remote(
            halo_sent.at[side], halo_came.at[side], halo_send.at[side], halo_recv.at[side], target
        ).wait_recv()
    loads[13].wait()
    loads[14].wait()
    has_left = (me > 0).astype(f32)
    has_right = (me < n - 1).astype(f32)
    for s in range(n):
        cols = slice(s * group, (s + 1) * group)
        before = halo_came[0, :, cols].astype(f32) * has_left
        after = halo_came[1, :, cols].astype(f32) * has_right
        parts = []
        for i, (r, taps) in enumerate(((gate, taps_gate), (mult, taps_mult), (value, taps_value))):
            parts.append(
                short_form(r[:, cols].astype(f32), taps[:, cols], before[i : i + 1], after[i : i + 1])
            )
        gate_part[s] = parts[0]
        direct[s] = skip_ref[:, cols] * (parts[1] * parts[2])
    loads[15].wait()

    def project(owner, convolved):
        gated = ((convolved + direct[owner]) * gate_part[owner]).astype(bf16)
        return mul(gated, weight[columns(owner), :])

    total[...] = project(me, own_back)
    for i, peer in enumerate(reversed(peers)):
        for h in range(PARTS):
            remote(
                back_sent.at[h, peer],
                back_came.at[h, peer],
                back_send.at[h, peer],
                back_recv.at[h, peer],
                peer,
            ).wait_recv()
        arrived = [back_came[h, peer].astype(f32) for h in range(PARTS)]
        term = project(peer, jnp.concatenate(arrived, axis=1))
        if i < n - 2:
            total[...] += term
        else:
            out_ref[0] = (total[...] + term).astype(bf16)
    for copy in copies:
        copy.wait_send()


def fused_body(n, *args):
    gate_in, mult_in, value_in, tg, tm, tv, first, second, ahead, behind, decay, skip, weight = args
    _, rows, channels = gate_in.shape
    seq_len, group = (rows * n, channels // n)
    width = weight.shape[1]
    part = group // PARTS
    tables, turn = wave_tables(seq_len)
    features = feature_table(seq_len, first.shape[0])
    vmem = pl.BlockSpec(memory_space=pltpu.VMEM)
    main = pl.BlockSpec(memory_space=pltpu.HBM)
    hidden_count = second.shape[0]
    dma = pltpu.SemaphoreType.DMA
    return pl.pallas_call(
        functools.partial(conv_kernel, n),
        out_shape=pltpu.VMEM((1, rows, width), bf16),
        in_specs=[main] * 16,
        out_specs=vmem,
        scratch_shapes=[
            pltpu.VMEM((rows, channels), bf16),
            pltpu.VMEM((rows, channels), bf16),
            pltpu.VMEM((rows, channels), bf16),
            pltpu.VMEM(tg.shape, f32),
            pltpu.VMEM(tm.shape, f32),
            pltpu.VMEM(tv.shape, f32),
            pltpu.VMEM(second.shape, f32),
            pltpu.VMEM((1, channels), f32),
            pltpu.VMEM((1, channels), f32),
            pltpu.VMEM((128, hidden_count), f32),
            pltpu.VMEM((hidden_count, group), f32),
            pltpu.VMEM((hidden_count, group), f32),
            pltpu.VMEM(weight.shape, bf16),
            pltpu.VMEM(tables.shape, bf16),
            pltpu.VMEM(turn.shape, f32),
            pltpu.VMEM(features.shape, f32),
            pltpu.VMEM((PARTS, n, rows + EDGE, part), bf16),
            pltpu.VMEM((PARTS, n, rows + EDGE, part), bf16),
            pltpu.VMEM((PARTS, seq_len, part), bf16),
            pltpu.VMEM((PARTS, n, rows, part), bf16),
            pltpu.VMEM((PARTS, n, rows, part), bf16),
            pltpu.VMEM((2, EDGE, channels), bf16),
            pltpu.VMEM((2, EDGE, channels), bf16),
            pltpu.VMEM((seq_len, group), f32),
            pltpu.VMEM((seq_len, group), f32),
            pltpu.VMEM((PARTS, 4, seq_len, part), bf16),
            pltpu.VMEM((n, rows, group), f32),
            pltpu.VMEM((n, rows, group), f32),
            pltpu.VMEM((rows, width), f32),
            dma((16,)),
            dma((PARTS, n)),
            dma((PARTS, n)),
            dma((PARTS, n)),
            dma((PARTS, n)),
            dma((2,)),
            dma((2,)),
        ],
        compiler_params=pltpu.CompilerParams(
            collective_id=0, has_side_effects=True, vmem_limit_bytes=61 * 1024 * 1024
        ),
    )(
        gate_in, mult_in, value_in, tg, tm, tv, first, second, ahead, behind,
        decay.reshape(1, channels), skip.reshape(1, channels), weight,
        jnp.asarray(tables), jnp.asarray(turn), jnp.asarray(features),
    )


def body_for(n, *args):
    _, rows, channels = args[0].shape
    small = rows * n <= 1024 and rows % 128 == 0 and channels % (128 * PARTS * n) == 0
    network = args[6].shape[0] <= 128 and args[6].shape[1] == 128
    if n >= 2 and n % 2 == 0 and small and network and args[3].shape[0] == 3:
        return fused_body(n, *args)
    return spread_body(*args)


def solution(mesh):
    in_specs = (
        P(("grp", "row"), "col", None),
        P(("grp", "row"), "col", None),
        P(("grp", "row"), "col", None),
        P(),
        P(),
        P(),
        P(),
        P(),
        P(),
        P(),
        P(),
        P(),
        P(),
    )
    out_specs = P(("grp", "row"), "col", None)

    body = functools.partial(body_for, mesh.shape["col"])
    return jax.shard_map(body, mesh=mesh, in_specs=in_specs, out_specs=out_specs, check_vma=False)
```

profile of v0, /device:TPU:0, one launch (start us, length us, event | category | flops | bytes accessed | tf_op | source)
XLA Modules:
  0.0 15.1 jit_solution(15113977907061531001)
XLA Ops:
  0.0 14.3 %shard_map.154 = bf16[1,128,2048]{2,1,0:T(8,128)(2,1)S(1)} custom-call(bf16[1,128,1024]{2,1,0:T(8,128)(2,1)} %gate_hbm.1, bf16[1,128,1024]{2,1,0:T(8,128)(2,1)} %mult_hbm.1, bf16[1,128,1024]{2,1,0:T(8,128)(2,1)} %value_hbm.1, f32[3,1024]{1,0:T(4,128)} %taps_gate_hbm.1, f32[3,1024]{1,0:T(4,128)} %taps_mult_hbm.1, f32[3,1024]{1,0:T(4,128)} %taps_value_hbm.1, ...), custom_call_target="tpu_custom_call" | custom-call | tf_op jit(solution)/shard_map/pallas_call | solution.py:556
  14.3 0.8 %copy.18 = bf16[1,128,2048]{2,1,0:T(8,128)(2,1)} copy(bf16[1,128,2048]{2,1,0:T(8,128)(2,1)S(1)} %shard_map.154) | data formatting | bytes 1048576
where the time goes:
time: 15.2 us; the launch traced here: 15.1 us
  Pallas kernels  14.3 us (94%)
  local copies, waits for them, and re-layouts  0.8 us (5%)
    pallas_call x1, Pallas kernels, fused_body(): pl.pallas_call(functools.partial(conv_kernel, n), out_shape=pltpu.VMEM((1...  14.3 us
    unnamed x1, local copies, waits for them, and re-layouts  0.8 us

commit v1 on v0

--- a/solution.py
+++ b/solution.py
@@ -185,19 +185,24 @@
 f32, bf16 = (jnp.float32, jnp.bfloat16)
 EDGE = 16
 PARTS = 2
+LANES = 128
+FEATS = 64
+
+
+def halves(table):
+    high = table.astype(bf16)
+    return [high, (table - high.astype(np.float64)).astype(bf16)]
 
 
 def wave_tables(seq_len):
     odd = 2 * np.arange(seq_len, dtype=np.int64) + 1
-    angle = (odd[:, None] * odd[None, :] % (8 * seq_len)) * (math.pi / (4 * seq_len))
-    pieces = []
-    for table in (np.cos(angle), np.sin(angle)):
-        high = table.astype(bf16)
-        pieces += [high, (table - high.astype(np.float64)).astype(bf16)]
-    half = odd * (math.pi / (4 * seq_len))
+    low = odd[: seq_len // 2]
+    angle = (low[:, None] * odd[None, :] % (8 * seq_len)) * (math.pi / (4 * seq_len))
+    table = np.concatenate([np.cos(angle), np.sin(angle)], axis=0)
+    half = low * (math.pi / (4 * seq_len))
     turn = np.stack([np.cos(half), np.sin(half)]).astype(np.float32)
-    turn = np.repeat(turn[:, :, None], 128, axis=2)
-    return (np.stack(pieces), turn)
+    turn = np.repeat(turn[:, :, None], LANES, axis=2)
+    return (np.stack(halves(table)), np.stack(halves(table.T)), turn)
 
 
 def feature_table(seq_len, feature_count):
@@ -207,7 +212,7 @@
     angles = (2.0 * math.pi / seq_len * position)[:, None] * values[None, :]
     tau = position / (seq_len - 1)
     table = np.concatenate([tau[:, None], np.cos(angles), -np.sin(angles)], axis=1)
-    return np.pad(table, ((0, 0), (0, 128 - feature_count))).astype(np.float32)
+    return np.concatenate(halves(np.pad(table, ((0, 0), (0, FEATS - feature_count)))), axis=1)
 
 
 def sine(x):
@@ -233,8 +238,13 @@
     return jnp.dot(a, b, preferred_element_type=f32)
 
 
-def mul_precise(a, b):
-    return jnp.dot(a, b, preferred_element_type=f32, precision=highest)
+def joined(value, axis):
+    return jnp.concatenate(split(value), axis=axis)
+
+
+def twice(weight):
+    both = joined(weight, 1)
+    return jnp.concatenate([both, both], axis=0)
 
 
 def neighbours(rows, before, after):
@@ -266,6 +276,7 @@
     skip_hbm,
     weight_hbm,
     table_hbm,
+    table_t_hbm,
     turn_hbm,
     feature_hbm,
     out_ref,
@@ -283,6 +294,7 @@
     behind_w,
     weight,
     table,
+    table_t,
     turn,
     feature,
     sent,
@@ -299,6 +311,7 @@
     direct,
     total,
     load_sems,
+    lead_sems,
     send_sems,
     recv_sems,
     back_send,
@@ -310,47 +323,54 @@
     rows, channels = gate.shape
     group = channels // n
     seq_len = rows * n
+    half = seq_len // 2
     near = me + 1 - 2 * lax.rem(me, 2)
     peers = []
     for j in range(1, n // 2):
         peers += [lax.rem(me + 2 * j, n), lax.rem(near + 2 * j, n)]
     peers.append(near)
-
-    def columns(owner):
-        return pl.ds(pl.multiple_of(owner * group, group), group)
-
-    loads = [
-        pltpu.make_async_copy(s, d, load_sems.at[i])
-        for i, (s, d) in enumerate(
-            [
-                (value_hbm.at[0], value),
-                (mult_hbm.at[0], mult),
-                (taps_value_hbm, taps_value),
-                (taps_mult_hbm, taps_mult),
-                (feature_hbm, feature),
-                (first_hbm, first.at[pl.ds(0, first_hbm.shape[0])]),
-                (second_hbm, second_ref),
-                (decay_hbm, decay_ref),
-                (ahead_hbm.at[:, columns(me)], ahead_w),
-                (behind_hbm.at[:, columns(me)], behind_w),
-                (table_hbm, table),
-                (turn_hbm, turn),
-                (gate_hbm.at[0], gate),
-                (taps_gate_hbm, taps_gate),
-                (skip_hbm, skip_ref),
-                (weight_hbm, weight),
-            ]
-        )
-    ]
-    for load in loads:
-        load.start()
+    order = peers + [me]
+
     barrier = pltpu.get_barrier_semaphore()
     for peer in peers:
         pl.semaphore_signal(
             barrier, inc=1, device_id={"col": peer}, device_id_type=pl.DeviceIdType.MESH
         )
-    for load in loads[:4]:
-        load.wait()
+
+    def columns(owner):
+        return pl.ds(pl.multiple_of(owner * group, group), group)
+
+    def load(src, dst, sem):
+        copy = pltpu.make_async_copy(src, dst, sem)
+        copy.start()
+        return copy
+
+    tap_loads = [
+        load(taps_value_hbm, taps_value, load_sems.at[0]),
+        load(taps_mult_hbm, taps_mult, load_sems.at[1]),
+    ]
+    lead = []
+    for i, owner in enumerate(order):
+        cols = columns(owner)
+        lead.append(
+            [
+                load(value_hbm.at[0, :, cols], value.at[:, cols], lead_sems.at[0, i]),
+                load(mult_hbm.at[0, :, cols], mult.at[:, cols], lead_sems.at[1, i]),
+            ]
+        )
+    loads = {}
+    for i, (name, s, d) in enumerate(
+        [
+            ("feature", feature_hbm, feature),
+            ("first", first_hbm, first.at[pl.ds(0, first_hbm.shape[0])]),
+            ("second", second_hbm, second_ref),
+            ("decay", decay_hbm, decay_ref),
+            ("ahead", ahead_hbm.at[:, columns(me)], ahead_w),
+            ("behind", behind_hbm.at[:, columns(me)], behind_w),
+            ("gate", gate_hbm.at[0], gate),
+        ]
+    ):
+        loads[name] = load(s, d, load_sems.at[2 + i])
 
     part = group // PARTS
 
@@ -381,8 +401,13 @@
         )
 
     copies = []
+    for copy in tap_loads:
+        copy.wait()
     for h in range(PARTS):
         for i, peer in enumerate(peers):
+            if h == 0:
+                for copy in lead[i]:
+                    copy.wait()
             pack(peer, h)
             if i + h == 0:
                 pl.semaphore_wait(barrier, n - 1)
@@ -391,14 +416,32 @@
             )
             copy.start()
             copies.append(copy)
-    loads[12].wait()
+    for i, (name, s, d) in enumerate(
+        [
+            ("table", table_hbm, table),
+            ("turn", turn_hbm, turn),
+            ("table_t", table_t_hbm, table_t),
+            ("taps_gate", taps_gate_hbm, taps_gate),
+            ("skip", skip_hbm, skip_ref),
+            ("weight", weight_hbm, weight),
+        ]
+    ):
+        loads[name] = load(s, d, load_sems.at[9 + i])
+    for copy in lead[n - 1]:
+        copy.wait()
+    loads["gate"].wait()
     right, left = (lax.rem(me + 1, n), lax.rem(me + n - 1, n))
+    slabs = channels // LANES
     for side, (row, target) in enumerate([(rows - 1, right), (0, left)]):
         base = rows - EDGE if row else 0
         at = row - base
-        parts = [r[base : base + EDGE, :].astype(f32)[at : at + 1] for r in (gate, mult, value)]
-        tile = jnp.concatenate(parts + [jnp.zeros((EDGE - 3, channels), f32)], axis=0)
-        halo_sent[side] = tile.astype(bf16)
+        parts = []
+        for r in (gate, mult, value):
+            line = r[base : base + EDGE, :].astype(f32)[at : at + 1]
+            parts.append(
+                jnp.concatenate([line[:, b * LANES : (b + 1) * LANES] for b in range(slabs)], axis=0)
+            )
+        halo_sent[side] = jnp.concatenate(parts, axis=1).astype(bf16)
         copy = remote(
             halo_sent.at[side], halo_came.at[side], halo_send.at[side], halo_recv.at[side], target
         )
@@ -407,44 +450,67 @@
     for h in range(PARTS):
         pack(me, h)
 
-    for load in loads[4:10]:
-        load.wait()
+    def signs(shape):
+        return (1 - 2 * (lax.broadcasted_iota(jnp.int32, shape, 0) % 2)).astype(f32)
+
+    for name in ("feature", "first", "second"):
+        loads[name].wait()
     used = first_hbm.shape[0]
     at = lax.broadcasted_iota(jnp.int32, first.shape, 0)
-    first_w = jnp.where(at < used, first[...], 0.0)
-    hidden = sine(mul_precise(feature[...], first_w))
-    hidden = sine(mul_precise(hidden, second_ref[...]))
-    later = pltpu.roll(hidden, seq_len - 1, 0)
-    rates = decay_ref[:, columns(me)]
+    wide = mul(feature[...], twice(jnp.where(at < used, first[...], 0.0)))
+    hidden = sine(wide[:, :LANES] + wide[:, LANES:])
+    wide = mul(joined(hidden, 1), twice(second_ref[...]))
+    hidden = sine(wide[:, :LANES] + wide[:, LANES:])
+    row_at = lax.broadcasted_iota(jnp.int32, hidden.shape, 0)
+    later = jnp.where(row_at == seq_len - 1, 0.0, pltpu.roll(hidden, seq_len - 1, 0))
+    for name in ("decay", "ahead", "behind"):
+        loads[name].wait()
+    rates = decay_ref[:, columns(me)] * (-1.0 / (seq_len - 1))
     index = lax.broadcasted_iota(jnp.int32, (seq_len, group), 0)
-    tau = index.astype(f32) * (1.0 / (seq_len - 1))
-    fade = jnp.exp(-rates * tau)
-    step = jnp.exp(-rates * (1.0 / (seq_len - 1)))
-    ahead = mul_precise(hidden, ahead_w[...]) * fade
-    behind = mul_precise(later, behind_w[...]) * (fade * step)
-    behind = jnp.where(index == seq_len - 1, 0.0, behind)
-    power = jnp.sum(ahead * ahead + behind * behind, axis=0, keepdims=True)
+    fade = jnp.exp(rates * index.astype(f32))
+
+    def side(values, w):
+        high, low = split(w)
+        return mul(values, jnp.concatenate([high, high], axis=0)) + mul(
+            values, jnp.concatenate([low, low], axis=0)
+        )
+
+    ahead = side(joined(hidden, 1), ahead_w[...])
+    behind = side(joined(later, 1), behind_w[...] * jnp.exp(rates))
+    sums = (ahead + behind) * fade
+    gaps = (ahead - behind) * fade
+    power = jnp.sum(sums * sums + gaps * gaps, axis=0, keepdims=True) * 0.5
     scale = lax.rsqrt(power + 1e-06) * (2.0 / (2 * seq_len))
-    loads[10].wait()
-    loads[11].wait()
-    high, low = split((ahead + behind) * scale)
-    even = mul(table[0], high) + mul(table[1], high) + mul(table[0], low)
-    high, low = split((ahead - behind) * scale)
-    odd = mul(table[2], high) + mul(table[3], high) + mul(table[2], low)
+    flip = signs((seq_len, part)).astype(bf16)
+    for name in ("table", "turn"):
+        loads[name].wait()
     cos_half = turn[0][:, 0:1]
     sin_half = turn[1][:, 0:1]
-    kernel_re[...] = cos_half * even + sin_half * odd
-    kernel_im[...] = sin_half * even - cos_half * odd
-
+    for h in range(PARTS):
+        cols = slice(h * part, (h + 1) * part)
+        sh, sl = split(sums[:, cols])
+        gh, gl = split(gaps[:, cols])
+
+        def turned(rows_at, a, b):
+            high = jnp.concatenate([a[0], b[0] * flip], axis=1)
+            low = jnp.concatenate([a[1], b[1] * flip], axis=1)
+            t0 = table[0, rows_at : rows_at + half, :]
+            t1 = table[1, rows_at : rows_at + half, :]
+            return mul(t0, high) + mul(t1, high) + mul(t0, low)
+
+        top = turned(0, (sh, sl), (gh, gl))
+        bottom = turned(half, (gh, gl), (sh, sl))
+        kernel_re[h] = cos_half * top + sin_half * bottom
+        kernel_im[h] = sin_half * top - cos_half * bottom
 
     def near_product(h):
-        whole[h, pl.ds(pl.multiple_of(me * rows, rows), rows), :] = sent[h, me, pl.ds(0, rows), :]
+        whole[h, pl.ds(pl.multiple_of(me * rows, rows), rows), :part] = sent[h, me, pl.ds(0, rows), :]
         came[h, me, pl.ds(rows, EDGE), :] = sent[h, me, pl.ds(rows, EDGE), :]
         for peer in reversed(peers):
             remote(
                 sent.at[h, peer], came.at[h, peer], send_sems.at[h, peer], recv_sems.at[h, peer], peer
             ).wait_recv()
-            whole[h, pl.ds(pl.multiple_of(peer * rows, rows), rows), :] = came[
+            whole[h, pl.ds(pl.multiple_of(peer * rows, rows), rows), :part] = came[
                 h, peer, pl.ds(0, rows), :
             ]
         edges = [came[h, s, pl.ds(rows, EDGE), :].astype(f32) for s in range(n)]
@@ -462,27 +528,26 @@
                     last_row += taps[2:3] * edges[s + 1][4 * k : 4 * k + 1]
                 top, bottom = (top * first_row, bottom * last_row)
             for base, at, row in ((s * rows, 0, top), ((s + 1) * rows - EDGE, EDGE - 1, bottom)):
-                old = whole[h, base : base + EDGE, :].astype(f32)
-                whole[h, base : base + EDGE, :] = jnp.where(tile_at == at, row, old).astype(bf16)
+                old = whole[h, base : base + EDGE, :part].astype(f32)
+                whole[h, base : base + EDGE, :part] = jnp.where(tile_at == at, row, old).astype(bf16)
+
+    alternate = signs((rows, part))
 
     def invert(owner, h):
         take = pl.ds(pl.multiple_of(owner * rows, rows), rows)
-        ch, cl, sh, sl = (table[i, take, :] for i in range(4))
-        return (
-            mul(ch, spec[h, 0]) + mul(sh, spec[h, 2])
-            + mul(cl, spec[h, 0]) + mul(sl, spec[h, 2])
-            + mul(ch, spec[h, 1]) + mul(sh, spec[h, 3])
-        )
-
+        both = mul(table_t[0, take, :], spec[h])
+        back = both[:, :part] + alternate * both[:, part:]
+        return back * scale[:, h * part : (h + 1) * part]
+
+    loads["table_t"].wait()
     for h in range(PARTS):
         near_product(h)
-        x = whole[h]
-        xc = mul(table[0], x) + mul(table[1], x)
-        xs = mul(table[2], x) + mul(table[3], x)
-        cols = slice(h * part, (h + 1) * part)
-        kr, ki = (kernel_re[:, cols], kernel_im[:, cols])
-        spec[h, 0], spec[h, 1] = split(xc * kr + xs * ki)
-        spec[h, 2], spec[h, 3] = split(xs * kr - xc * ki)
+        whole[h, :, part:] = whole[h, :, :part] * flip
+        freq = mul(table[0], whole[h])
+        top, bottom = (freq[:half], freq[half:])
+        kr, ki = (kernel_re[h], kernel_im[h])
+        spec[h, :half] = (top * kr + bottom * ki).astype(bf16)
+        spec[h, half:] = (bottom * kr - top * ki).astype(bf16)
         for peer in peers:
             back_sent[h, peer] = invert(peer, h).astype(bf16)
             copy = remote(
@@ -500,22 +565,28 @@
         remote(
             halo_sent.at[side], halo_came.at[side], halo_send.at[side], halo_recv.at[side], target
         ).wait_recv()
-    loads[13].wait()
-    loads[14].wait()
+    for name in ("taps_gate", "skip"):
+        loads[name].wait()
     has_left = (me > 0).astype(f32)
     has_right = (me < n - 1).astype(f32)
+    befores = halo_came[0].astype(f32) * has_left
+    afters = halo_came[1].astype(f32) * has_right
+
+    def line(halo, i, s):
+        lanes = slice(i * LANES, (i + 1) * LANES)
+        blocks = range(s * group // LANES, (s + 1) * group // LANES)
+        return jnp.concatenate([halo[b : b + 1, lanes] for b in blocks], axis=1)
+
     for s in range(n):
         cols = slice(s * group, (s + 1) * group)
-        before = halo_came[0, :, cols].astype(f32) * has_left
-        after = halo_came[1, :, cols].astype(f32) * has_right
         parts = []
         for i, (r, taps) in enumerate(((gate, taps_gate), (mult, taps_mult), (value, taps_value))):
             parts.append(
-                short_form(r[:, cols].astype(f32), taps[:, cols], before[i : i + 1], after[i : i + 1])
+                short_form(r[:, cols].astype(f32), taps[:, cols], line(befores, i, s), line(afters, i, s))
             )
         gate_part[s] = parts[0]
         direct[s] = skip_ref[:, cols] * (parts[1] * parts[2])
-    loads[15].wait()
+    loads["weight"].wait()
 
     def project(owner, convolved):
         gated = ((convolved + direct[owner]) * gate_part[owner]).astype(bf16)
@@ -547,7 +618,8 @@
     seq_len, group = (rows * n, channels // n)
     width = weight.shape[1]
     part = group // PARTS
-    tables, turn = wave_tables(seq_len)
+    slabs = channels // LANES
+    table, table_t, turn = wave_tables(seq_len)
     features = feature_table(seq_len, first.shape[0])
     vmem = pl.BlockSpec(memory_space=pltpu.VMEM)
     main = pl.BlockSpec(memory_space=pltpu.HBM)
@@ -556,7 +628,7 @@
     return pl.pallas_call(
         functools.partial(conv_kernel, n),
         out_shape=pltpu.VMEM((1, rows, width), bf16),
-        in_specs=[main] * 16,
+        in_specs=[main] * 17,
         out_specs=vmem,
         scratch_shapes=[
             pltpu.VMEM((rows, channels), bf16),
@@ -568,27 +640,29 @@
             pltpu.VMEM(second.shape, f32),
             pltpu.VMEM((1, channels), f32),
             pltpu.VMEM((1, channels), f32),
-            pltpu.VMEM((128, hidden_count), f32),
+            pltpu.VMEM((FEATS, hidden_count), f32),
             pltpu.VMEM((hidden_count, group), f32),
             pltpu.VMEM((hidden_count, group), f32),
             pltpu.VMEM(weight.shape, bf16),
-            pltpu.VMEM(tables.shape, bf16),
+            pltpu.VMEM(table.shape, bf16),
+            pltpu.VMEM(table_t.shape, bf16),
             pltpu.VMEM(turn.shape, f32),
-            pltpu.VMEM(features.shape, f32),
+            pltpu.VMEM(features.shape, bf16),
             pltpu.VMEM((PARTS, n, rows + EDGE, part), bf16),
             pltpu.VMEM((PARTS, n, rows + EDGE, part), bf16),
-            pltpu.VMEM((PARTS, seq_len, part), bf16),
+            pltpu.VMEM((PARTS, seq_len, 2 * part), bf16),
             pltpu.VMEM((PARTS, n, rows, part), bf16),
             pltpu.VMEM((PARTS, n, rows, part), bf16),
-            pltpu.VMEM((2, EDGE, channels), bf16),
-            pltpu.VMEM((2, EDGE, channels), bf16),
-            pltpu.VMEM((seq_len, group), f32),
-            pltpu.VMEM((seq_len, group), f32),
-            pltpu.VMEM((PARTS, 4, seq_len, part), bf16),
+            pltpu.VMEM((2, slabs, 3 * LANES), bf16),
+            pltpu.VMEM((2, slabs, 3 * LANES), bf16),
+            pltpu.VMEM((PARTS, seq_len // 2, 2 * part), f32),
+            pltpu.VMEM((PARTS, seq_len // 2, 2 * part), f32),
+            pltpu.VMEM((PARTS, seq_len, 2 * part), bf16),
             pltpu.VMEM((n, rows, group), f32),
             pltpu.VMEM((n, rows, group), f32),
             pltpu.VMEM((rows, width), f32),
-            dma((16,)),
+            dma((15,)),
+            dma((2, n)),
             dma((PARTS, n)),
             dma((PARTS, n)),
             dma((PARTS, n)),
@@ -602,14 +676,14 @@
     )(
         gate_in, mult_in, value_in, tg, tm, tv, first, second, ahead, behind,
         decay.reshape(1, channels), skip.reshape(1, channels), weight,
-        jnp.asarray(tables), jnp.asarray(turn), jnp.asarray(features),
+        jnp.asarray(table), jnp.asarray(table_t), jnp.asarray(turn), jnp.asarray(features),
     )
 
 
 def body_for(n, *args):
     _, rows, channels = args[0].shape
     small = rows * n <= 1024 and rows % 128 == 0 and channels % (128 * PARTS * n) == 0
-    network = args[6].shape[0] <= 128 and args[6].shape[1] == 128
+    network = args[6].shape[0] <= FEATS and args[6].shape[1] == 128
     if n >= 2 and n % 2 == 0 and small and network and args[3].shape[0] == 3:
         return fused_body(n, *args)
     return spread_body(*args)

time: 15.2 us -> 14.5 us (0.954)
  Pallas kernels: 14.3 us -> 13.5 us
    pallas_call x1, Pallas kernels: 14.3 us -> 13.5 us  [fused_body(): pl.pallas_call(functools.partial(conv_kernel, n), out_shape=pltpu.VMEM((1...]
where the time goes in v1:
time: 14.5 us; the launch traced here: 14.3 us
  Pallas kernels  13.5 us (93%)
  local copies, waits for them, and re-layouts  0.8 us (6%)
    pallas_call x1, Pallas kernels, fused_body(): pl.pallas_call(functools.partial(conv_kernel, n), out_shape=pltpu.VMEM((1...  13.5 us
    unnamed x1, local copies, waits for them, and re-layouts  0.8 us

profile of v1, /device:TPU:0, one launch (start us, length us, event | category | flops | bytes accessed | tf_op | source)
XLA Modules:
  0.0 14.3 jit_solution(613679646948264474)
XLA Ops:
  0.0 13.5 %shard_map.163 = bf16[1,128,2048]{2,1,0:T(8,128)(2,1)S(1)} custom-call(bf16[1,128,1024]{2,1,0:T(8,128)(2,1)} %gate_hbm.1, bf16[1,128,1024]{2,1,0:T(8,128)(2,1)} %mult_hbm.1, bf16[1,128,1024]{2,1,0:T(8,128)(2,1)} %value_hbm.1, f32[3,1024]{1,0:T(4,128)} %taps_gate_hbm.1, f32[3,1024]{1,0:T(4,128)} %taps_mult_hbm.1, f32[3,1024]{1,0:T(4,128)} %taps_value_hbm.1, ...), custom_call_target="tpu_custom_call" | custom-call | tf_op jit(solution)/shard_map/pallas_call | solution.py:628
  13.5 0.8 %copy.19 = bf16[1,128,2048]{2,1,0:T(8,128)(2,1)} copy(bf16[1,128,2048]{2,1,0:T(8,128)(2,1)S(1)} %shard_map.163) | data formatting | bytes 1048576

commit v2 on v1

--- a/solution.py
+++ b/solution.py
@@ -184,7 +184,6 @@
 
 f32, bf16 = (jnp.float32, jnp.bfloat16)
 EDGE = 16
-PARTS = 2
 LANES = 128
 FEATS = 64
 
@@ -280,6 +279,7 @@
     turn_hbm,
     feature_hbm,
     out_ref,
+    rims,
     gate,
     mult,
     value,
@@ -297,13 +297,17 @@
     table_t,
     turn,
     feature,
+    halo_sent,
+    halo_came,
     sent,
     came,
-    whole,
+    wide_sent,
+    rim_sent,
+    wide_came,
     back_sent,
     back_came,
-    halo_sent,
-    halo_came,
+    near_sent,
+    near_came,
     kernel_re,
     kernel_im,
     spec,
@@ -311,25 +315,29 @@
     direct,
     total,
     load_sems,
-    lead_sems,
     send_sems,
     recv_sems,
+    wide_send,
+    wide_recv,
     back_send,
     back_recv,
+    near_sems,
     halo_send,
     halo_recv,
 ):
     me = lax.axis_index("col")
     rows, channels = gate.shape
-    group = channels // n
+    slabs = channels // LANES
+    share = (slabs - n) // 2
     seq_len = rows * n
     half = seq_len // 2
-    near = me + 1 - 2 * lax.rem(me, 2)
-    peers = []
+    core = lax.rem(me, 2)
+    near = me + 1 - 2 * core
+    far = []
     for j in range(1, n // 2):
-        peers += [lax.rem(me + 2 * j, n), lax.rem(near + 2 * j, n)]
-    peers.append(near)
-    order = peers + [me]
+        chip = lax.rem(me - core + 2 * j, n)
+        far += [chip, chip + 1]
+    peers = far + [near]
 
     barrier = pltpu.get_barrier_semaphore()
     for peer in peers:
@@ -337,58 +345,25 @@
             barrier, inc=1, device_id={"col": peer}, device_id_type=pl.DeviceIdType.MESH
         )
 
-    def columns(owner):
-        return pl.ds(pl.multiple_of(owner * group, group), group)
-
-    def load(src, dst, sem):
-        copy = pltpu.make_async_copy(src, dst, sem)
+    def lanes(slab, count=1):
+        start = slab * LANES
+        if not isinstance(slab, int):
+            start = pl.multiple_of(start, LANES)
+        return pl.ds(start, count * LANES)
+
+    def span(owner):
+        return pl.ds(pl.multiple_of(owner * rows, rows), rows)
+
+    loads = {}
+
+    def load(name, src, dst):
+        copy = pltpu.make_async_copy(src, dst, load_sems.at[len(loads)])
         copy.start()
-        return copy
-
-    tap_loads = [
-        load(taps_value_hbm, taps_value, load_sems.at[0]),
-        load(taps_mult_hbm, taps_mult, load_sems.at[1]),
-    ]
-    lead = []
-    for i, owner in enumerate(order):
-        cols = columns(owner)
-        lead.append(
-            [
-                load(value_hbm.at[0, :, cols], value.at[:, cols], lead_sems.at[0, i]),
-                load(mult_hbm.at[0, :, cols], mult.at[:, cols], lead_sems.at[1, i]),
-            ]
-        )
-    loads = {}
-    for i, (name, s, d) in enumerate(
-        [
-            ("feature", feature_hbm, feature),
-            ("first", first_hbm, first.at[pl.ds(0, first_hbm.shape[0])]),
-            ("second", second_hbm, second_ref),
-            ("decay", decay_hbm, decay_ref),
-            ("ahead", ahead_hbm.at[:, columns(me)], ahead_w),
-            ("behind", behind_hbm.at[:, columns(me)], behind_w),
-            ("gate", gate_hbm.at[0], gate),
-        ]
-    ):
-        loads[name] = load(s, d, load_sems.at[2 + i])
-
-    part = group // PARTS
-
-    def piece(owner, h):
-        return pl.ds(pl.multiple_of(owner * group + h * part, part), part)
-
-    def pack(owner, h):
-        cols = piece(owner, h)
-        v = value[:, cols].astype(f32)
-        m = mult[:, cols].astype(f32)
-        zero = jnp.zeros((1, part), f32)
-        vs = short_form(v, taps_value[:, cols], zero, zero)
-        ms = short_form(m, taps_mult[:, cols], zero, zero)
-        sent[h, owner, pl.ds(0, rows), :] = (vs * ms).astype(bf16)
-        edges = jnp.concatenate(
-            [v[0:2], v[rows - 2 : rows], m[0:2], m[rows - 2 : rows], jnp.zeros((8, part), f32)], axis=0
-        )
-        sent[h, owner, pl.ds(rows, EDGE), :] = edges.astype(bf16)
+        loads[name] = copy
+
+    def ready(*names):
+        for name in names:
+            loads[name].wait()
 
     def remote(src, dst, ssem, rsem, peer):
         return pltpu.make_async_remote_copy(
@@ -400,61 +375,104 @@
             device_id_type=pl.DeviceIdType.MESH,
         )
 
+    for side, base in enumerate((rows - EDGE, 0)):
+        for i, ref in enumerate((gate_hbm, mult_hbm, value_hbm)):
+            load(f"rim{side}{i}", ref.at[0, pl.ds(base, EDGE)], rims.at[side, i])
+    load("taps_value", taps_value_hbm, taps_value)
+    load("taps_mult", taps_mult_hbm, taps_mult)
+    for i, (low, count) in enumerate(((0, n), (n, slabs - n))):
+        load(f"value{i}", value_hbm.at[0, :, lanes(low, count)], value.at[:, lanes(low, count)])
+        load(f"mult{i}", mult_hbm.at[0, :, lanes(low, count)], mult.at[:, lanes(low, count)])
+    own_wide = n + share * core
+    load("feature", feature_hbm, feature)
+    load("first", first_hbm, first.at[pl.ds(0, first_hbm.shape[0])])
+    load("second", second_hbm, second_ref)
+    load("decay", decay_hbm, decay_ref)
+    for name, s, d in (("ahead", ahead_hbm, ahead_w), ("behind", behind_hbm, behind_w)):
+        load(name + "0", s.at[:, lanes(me)], d.at[:, lanes(0)])
+        load(name + "1", s.at[:, lanes(own_wide, share)], d.at[:, lanes(1, share)])
+
     copies = []
-    for copy in tap_loads:
-        copy.wait()
-    for h in range(PARTS):
-        for i, peer in enumerate(peers):
-            if h == 0:
-                for copy in lead[i]:
-                    copy.wait()
-            pack(peer, h)
-            if i + h == 0:
-                pl.semaphore_wait(barrier, n - 1)
-            copy = remote(
-                sent.at[h, peer], came.at[h, me], send_sems.at[h, peer], recv_sems.at[h, me], peer
-            )
-            copy.start()
-            copies.append(copy)
-    for i, (name, s, d) in enumerate(
-        [
-            ("table", table_hbm, table),
-            ("turn", turn_hbm, turn),
-            ("table_t", table_t_hbm, table_t),
-            ("taps_gate", taps_gate_hbm, taps_gate),
-            ("skip", skip_hbm, skip_ref),
-            ("weight", weight_hbm, weight),
-        ]
-    ):
-        loads[name] = load(s, d, load_sems.at[9 + i])
-    for copy in lead[n - 1]:
-        copy.wait()
-    loads["gate"].wait()
+
+    def send(*args):
+        copy = remote(*args)
+        copy.start()
+        copies.append(copy)
+
+    ready(*(f"rim{side}{i}" for side in range(2) for i in range(3)))
     right, left = (lax.rem(me + 1, n), lax.rem(me + n - 1, n))
-    slabs = channels // LANES
-    for side, (row, target) in enumerate([(rows - 1, right), (0, left)]):
-        base = rows - EDGE if row else 0
-        at = row - base
+    for side, at in enumerate((EDGE - 1, 0)):
         parts = []
-        for r in (gate, mult, value):
-            line = r[base : base + EDGE, :].astype(f32)[at : at + 1]
+        for i in range(3):
+            line = rims[side, i].astype(f32)[at : at + 1]
             parts.append(
                 jnp.concatenate([line[:, b * LANES : (b + 1) * LANES] for b in range(slabs)], axis=0)
             )
         halo_sent[side] = jnp.concatenate(parts, axis=1).astype(bf16)
-        copy = remote(
+    pl.semaphore_wait(barrier, n - 1)
+    for side, target in enumerate((right, left)):
+        send(
             halo_sent.at[side], halo_came.at[side], halo_send.at[side], halo_recv.at[side], target
         )
-        copy.start()
-        copies.append(copy)
-    for h in range(PARTS):
-        pack(me, h)
+
+    zero = jnp.zeros((1, LANES), f32)
+
+    def short_product(v, m, slab):
+        vs = short_form(v, taps_value[:, lanes(slab)], zero, zero)
+        ms = short_form(m, taps_mult[:, lanes(slab)], zero, zero)
+        return (vs * ms).astype(bf16)
+
+    def pack(owner):
+        v = value[:, lanes(owner)].astype(f32)
+        m = mult[:, lanes(owner)].astype(f32)
+        sent[owner, pl.ds(0, rows), :] = short_product(v, m, owner)
+        edges = [v[0:2], v[rows - 2 : rows], m[0:2], m[rows - 2 : rows], jnp.zeros((8, LANES), f32)]
+        sent[owner, pl.ds(rows, EDGE), :] = jnp.concatenate(edges, axis=0).astype(bf16)
+
+    ready("taps_value", "taps_mult", "value0", "mult0")
+    for peer in peers:
+        pack(peer)
+        send(sent.at[peer], came.at[me], send_sems.at[peer], recv_sems.at[me], peer)
+    pack(me)
+
+    ready("value1", "mult1")
+    for slab in range(n, slabs):
+        cols = lanes(slab)
+        wide_sent[slab - n] = short_product(value[:, cols].astype(f32), mult[:, cols].astype(f32), slab)
+    inner = pl.ds(EDGE, rows - 2 * EDGE)
+
+    def inner_of(owner):
+        return pl.ds(pl.multiple_of(owner * rows + EDGE, EDGE), rows - 2 * EDGE)
+
+    def rim_of(owner, side):
+        return pl.ds(pl.multiple_of(owner * rows + (1 - side) * (rows - EDGE), EDGE), EDGE)
+
+    def own_share(peer):
+        return pl.ds(lax.rem(peer, 2) * share, share)
+
+    for peer in peers:
+        send(
+            wide_sent.at[own_share(peer), inner],
+            wide_came.at[:, inner_of(me)],
+            wide_send.at[0, peer],
+            wide_recv.at[0, me],
+            peer,
+        )
+    for j in range(share):
+        wide_came[j, inner_of(me), :] = wide_sent[core * share + j, inner, :]
+
+    load("table", table_hbm, table)
+    load("turn", turn_hbm, turn)
+    load("table_t", table_t_hbm, table_t)
+    load("gate", gate_hbm.at[0], gate)
+    load("taps_gate", taps_gate_hbm, taps_gate)
+    load("skip", skip_hbm, skip_ref)
+    load("weight", weight_hbm, weight)
 
     def signs(shape):
         return (1 - 2 * (lax.broadcasted_iota(jnp.int32, shape, 0) % 2)).astype(f32)
 
-    for name in ("feature", "first", "second"):
-        loads[name].wait()
+    ready("feature", "first", "second")
     used = first_hbm.shape[0]
     at = lax.broadcasted_iota(jnp.int32, first.shape, 0)
     wide = mul(feature[...], twice(jnp.where(at < used, first[...], 0.0)))
@@ -463,31 +481,30 @@
     hidden = sine(wide[:, :LANES] + wide[:, LANES:])
     row_at = lax.broadcasted_iota(jnp.int32, hidden.shape, 0)
     later = jnp.where(row_at == seq_len - 1, 0.0, pltpu.roll(hidden, seq_len - 1, 0))
-    for name in ("decay", "ahead", "behind"):
-        loads[name].wait()
-    rates = decay_ref[:, columns(me)] * (-1.0 / (seq_len - 1))
-    index = lax.broadcasted_iota(jnp.int32, (seq_len, group), 0)
+    ready("decay", "ahead0", "ahead1", "behind0", "behind1")
+    both_rates = [decay_ref[:, lanes(me)], decay_ref[:, lanes(own_wide, share)]]
+    rates = jnp.concatenate(both_rates, axis=1) * (-1.0 / (seq_len - 1))
+    index = lax.broadcasted_iota(jnp.int32, (seq_len, (1 + share) * LANES), 0)
     fade = jnp.exp(rates * index.astype(f32))
 
-    def side(values, w):
+    def side_of(values, w):
         high, low = split(w)
         return mul(values, jnp.concatenate([high, high], axis=0)) + mul(
             values, jnp.concatenate([low, low], axis=0)
         )
 
-    ahead = side(joined(hidden, 1), ahead_w[...])
-    behind = side(joined(later, 1), behind_w[...] * jnp.exp(rates))
+    ahead = side_of(joined(hidden, 1), ahead_w[...])
+    behind = side_of(joined(later, 1), behind_w[...] * jnp.exp(rates))
     sums = (ahead + behind) * fade
     gaps = (ahead - behind) * fade
     power = jnp.sum(sums * sums + gaps * gaps, axis=0, keepdims=True) * 0.5
     scale = lax.rsqrt(power + 1e-06) * (2.0 / (2 * seq_len))
-    flip = signs((seq_len, part)).astype(bf16)
-    for name in ("table", "turn"):
-        loads[name].wait()
+    flip = signs((seq_len, LANES)).astype(bf16)
+    ready("table", "turn")
     cos_half = turn[0][:, 0:1]
     sin_half = turn[1][:, 0:1]
-    for h in range(PARTS):
-        cols = slice(h * part, (h + 1) * part)
+    for j in range(1 + share):
+        cols = slice(j * LANES, (j + 1) * LANES)
         sh, sl = split(sums[:, cols])
         gh, gl = split(gaps[:, cols])
 
@@ -500,114 +517,142 @@
 
         top = turned(0, (sh, sl), (gh, gl))
         bottom = turned(half, (gh, gl), (sh, sl))
-        kernel_re[h] = cos_half * top + sin_half * bottom
-        kernel_im[h] = sin_half * top - cos_half * bottom
-
-    def near_product(h):
-        whole[h, pl.ds(pl.multiple_of(me * rows, rows), rows), :part] = sent[h, me, pl.ds(0, rows), :]
-        came[h, me, pl.ds(rows, EDGE), :] = sent[h, me, pl.ds(rows, EDGE), :]
-        for peer in reversed(peers):
-            remote(
-                sent.at[h, peer], came.at[h, peer], send_sems.at[h, peer], recv_sems.at[h, peer], peer
-            ).wait_recv()
-            whole[h, pl.ds(pl.multiple_of(peer * rows, rows), rows), :part] = came[
-                h, peer, pl.ds(0, rows), :
-            ]
-        edges = [came[h, s, pl.ds(rows, EDGE), :].astype(f32) for s in range(n)]
-        own_taps = [t[:, piece(me, h)] for t in (taps_value, taps_mult)]
-        tile_at = lax.broadcasted_iota(jnp.int32, (EDGE, part), 0)
-        for s in range(n):
-            top = bottom = 1.0
-            for k, taps in enumerate(own_taps):
-                e = edges[s][4 * k : 4 * k + 4]
-                first_row = taps[1:2] * e[0:1] + taps[2:3] * e[1:2]
-                last_row = taps[0:1] * e[2:3] + taps[1:2] * e[3:4]
-                if s > 0:
-                    first_row += taps[0:1] * edges[s - 1][4 * k + 3 : 4 * k + 4]
-                if s < n - 1:
-                    last_row += taps[2:3] * edges[s + 1][4 * k : 4 * k + 1]
-                top, bottom = (top * first_row, bottom * last_row)
-            for base, at, row in ((s * rows, 0, top), ((s + 1) * rows - EDGE, EDGE - 1, bottom)):
-                old = whole[h, base : base + EDGE, :part].astype(f32)
-                whole[h, base : base + EDGE, :part] = jnp.where(tile_at == at, row, old).astype(bf16)
-
-    alternate = signs((rows, part))
-
-    def invert(owner, h):
-        take = pl.ds(pl.multiple_of(owner * rows, rows), rows)
-        both = mul(table_t[0, take, :], spec[h])
-        back = both[:, :part] + alternate * both[:, part:]
-        return back * scale[:, h * part : (h + 1) * part]
-
-    loads["table_t"].wait()
-    for h in range(PARTS):
-        near_product(h)
-        whole[h, :, part:] = whole[h, :, :part] * flip
-        freq = mul(table[0], whole[h])
-        top, bottom = (freq[:half], freq[half:])
-        kr, ki = (kernel_re[h], kernel_im[h])
-        spec[h, :half] = (top * kr + bottom * ki).astype(bf16)
-        spec[h, half:] = (bottom * kr - top * ki).astype(bf16)
-        for peer in peers:
-            back_sent[h, peer] = invert(peer, h).astype(bf16)
-            copy = remote(
-                back_sent.at[h, peer],
-                back_came.at[h, me],
-                back_send.at[h, peer],
-                back_recv.at[h, me],
-                peer,
-            )
-            copy.start()
-            copies.append(copy)
-    own_back = jnp.concatenate([invert(me, h) for h in range(PARTS)], axis=1)
-
-    for side, target in enumerate((left, right)):
+        kernel_re[j] = cos_half * top + sin_half * bottom
+        kernel_im[j] = sin_half * top - cos_half * bottom
+
+    for side, target in enumerate((right, left)):
         remote(
             halo_sent.at[side], halo_came.at[side], halo_send.at[side], halo_recv.at[side], target
         ).wait_recv()
-    for name in ("taps_gate", "skip"):
-        loads[name].wait()
-    has_left = (me > 0).astype(f32)
-    has_right = (me < n - 1).astype(f32)
-    befores = halo_came[0].astype(f32) * has_left
-    afters = halo_came[1].astype(f32) * has_right
-
-    def line(halo, i, s):
-        lanes = slice(i * LANES, (i + 1) * LANES)
-        blocks = range(s * group // LANES, (s + 1) * group // LANES)
-        return jnp.concatenate([halo[b : b + 1, lanes] for b in blocks], axis=1)
-
+    befores = halo_came[0].astype(f32) * (me > 0).astype(f32)
+    afters = halo_came[1].astype(f32) * (me < n - 1).astype(f32)
+
+    def line_of(halo, i, slab):
+        return halo[slab : slab + 1, i * LANES : (i + 1) * LANES]
+
+    rim_at = lax.broadcasted_iota(jnp.int32, (EDGE, LANES), 0)
+    for slab in range(n, slabs):
+        first_row = last_row = 1.0
+        for i, taps in ((1, taps_mult), (2, taps_value)):
+            t = taps[:, lanes(slab)]
+            upper = rims[1, i, :, lanes(slab)].astype(f32)
+            lower = rims[0, i, :, lanes(slab)].astype(f32)
+            first_row *= (
+                t[0:1] * line_of(befores, i, slab) + t[1:2] * upper[0:1] + t[2:3] * upper[1:2]
+            )
+            last_row *= (
+                t[0:1] * lower[EDGE - 2 : EDGE - 1]
+                + t[1:2] * lower[EDGE - 1 : EDGE]
+                + t[2:3] * line_of(afters, i, slab)
+            )
+        for side, row, where in ((1, first_row, 0), (0, last_row, EDGE - 1)):
+            base = 0 if side else rows - EDGE
+            old = wide_sent[slab - n, base : base + EDGE, :].astype(f32)
+            rim_sent[side, slab - n] = jnp.where(rim_at == where, row, old).astype(bf16)
+    for peer in peers:
+        for side in range(2):
+            send(
+                rim_sent.at[side, own_share(peer)],
+                wide_came.at[:, rim_of(me, side)],
+                wide_send.at[1 + side, peer],
+                wide_recv.at[1 + side, me],
+                peer,
+            )
+    for j in range(share):
+        for side in range(2):
+            wide_came[j, rim_of(me, side), :] = rim_sent[side, core * share + j]
+
+    alternate = signs((rows, LANES))
+
+    def convolve(j, x):
+        freq = mul(table[0], jnp.concatenate([x, x * flip], axis=1))
+        top, bottom = (freq[:half], freq[half:])
+        kr, ki = (kernel_re[j], kernel_im[j])
+        spec[j, :half] = (top * kr + bottom * ki).astype(bf16)
+        spec[j, half:] = (bottom * kr - top * ki).astype(bf16)
+
+    def invert(owner, j):
+        both = mul(table_t[0, span(owner), :], spec[j])
+        back = both[:, :LANES] + alternate * both[:, LANES:]
+        return back * scale[:, j * LANES : (j + 1) * LANES]
+
+    came[me] = sent[me]
+    for peer in reversed(peers):
+        remote(
+            sent.at[peer], came.at[peer], send_sems.at[peer], recv_sems.at[peer], peer
+        ).wait_recv()
+    edges = [came[s, pl.ds(rows, EDGE), :].astype(f32) for s in range(n)]
+    own_taps = [t[:, lanes(me)] for t in (taps_value, taps_mult)]
+    pieces = []
     for s in range(n):
-        cols = slice(s * group, (s + 1) * group)
+        top = bottom = 1.0
+        for k, taps in enumerate(own_taps):
+            e = edges[s][4 * k : 4 * k + 4]
+            first_row = taps[1:2] * e[0:1] + taps[2:3] * e[1:2]
+            last_row = taps[0:1] * e[2:3] + taps[1:2] * e[3:4]
+            if s > 0:
+                first_row += taps[0:1] * edges[s - 1][4 * k + 3 : 4 * k + 4]
+            if s < n - 1:
+                last_row += taps[2:3] * edges[s + 1][4 * k : 4 * k + 1]
+            top, bottom = (top * first_row, bottom * last_row)
+        block = came[s, pl.ds(0, rows), :]
+        upper = jnp.where(rim_at == 0, top, block[:EDGE].astype(f32)).astype(bf16)
+        lower = jnp.where(rim_at == EDGE - 1, bottom, block[rows - EDGE :].astype(f32)).astype(bf16)
+        pieces += [upper, block[EDGE : rows - EDGE], lower]
+    ready("table_t")
+    convolve(0, jnp.concatenate(pieces, axis=0))
+    for peer in peers:
+        back_sent[peer] = invert(peer, 0).astype(bf16)
+        send(back_sent.at[peer], back_came.at[me], back_send.at[peer], back_recv.at[me], peer)
+    own_back = invert(me, 0)
+
+    ready("gate", "taps_gate", "skip")
+    for slab in range(slabs):
+        cols = lanes(slab)
         parts = []
         for i, (r, taps) in enumerate(((gate, taps_gate), (mult, taps_mult), (value, taps_value))):
             parts.append(
-                short_form(r[:, cols].astype(f32), taps[:, cols], line(befores, i, s), line(afters, i, s))
+                short_form(
+                    r[:, cols].astype(f32), taps[:, cols], line_of(befores, i, slab), line_of(afters, i, slab)
+                )
             )
-        gate_part[s] = parts[0]
-        direct[s] = skip_ref[:, cols] * (parts[1] * parts[2])
-    loads["weight"].wait()
-
-    def project(owner, convolved):
-        gated = ((convolved + direct[owner]) * gate_part[owner]).astype(bf16)
-        return mul(gated, weight[columns(owner), :])
-
-    total[...] = project(me, own_back)
-    for i, peer in enumerate(reversed(peers)):
-        for h in range(PARTS):
+        gate_part[slab] = parts[0]
+        direct[slab] = skip_ref[:, cols] * (parts[1] * parts[2])
+    ready("weight")
+
+    def gated(slab, convolved):
+        return ((convolved + direct[slab]) * gate_part[slab]).astype(bf16)
+
+    def project(items):
+        left_side = jnp.concatenate([gated(slab, value) for slab, value in items], axis=1)
+        return mul(left_side, jnp.concatenate([weight[lanes(slab), :] for slab, _ in items], axis=0))
+
+    def returned(peer):
+        remote(
+            back_sent.at[peer], back_came.at[peer], back_send.at[peer], back_recv.at[peer], peer
+        ).wait_recv()
+        return (peer, back_came[peer].astype(f32))
+
+    for peer in reversed(peers):
+        for i in range(3):
+            where = inner_of(peer) if i == 0 else rim_of(peer, i - 1)
+            what = wide_sent.at[own_share(me), inner] if i == 0 else rim_sent.at[i - 1, own_share(me)]
             remote(
-                back_sent.at[h, peer],
-                back_came.at[h, peer],
-                back_send.at[h, peer],
-                back_recv.at[h, peer],
-                peer,
+                what, wide_came.at[:, where], wide_send.at[i, peer], wide_recv.at[i, peer], peer
             ).wait_recv()
-        arrived = [back_came[h, peer].astype(f32) for h in range(PARTS)]
-        term = project(peer, jnp.concatenate(arrived, axis=1))
-        if i < n - 2:
-            total[...] += term
-        else:
-            out_ref[0] = (total[...] + term).astype(bf16)
+    for j in range(share):
+        convolve(1 + j, wide_came[j])
+    for j in range(share):
+        near_sent[j] = invert(near, 1 + j).astype(bf16)
+    send(near_sent, near_came, near_sems.at[0], near_sems.at[1], near)
+    items = [(own_wide + j, invert(me, 1 + j)) for j in range(share)]
+    items += [(me, own_back), returned(near)]
+    total[...] = project(items)
+    items = [returned(peer) for peer in reversed(far)]
+    remote(near_sent, near_came, near_sems.at[0], near_sems.at[1], near).wait_recv()
+    near_wide = n + share * (1 - core)
+    items += [(near_wide + j, near_came[j].astype(f32)) for j in range(share)]
+    out_ref[0] = (total[...] + project(items)).astype(bf16)
     for copy in copies:
         copy.wait_send()
 
@@ -615,11 +660,13 @@
 def fused_body(n, *args):
     gate_in, mult_in, value_in, tg, tm, tv, first, second, ahead, behind, decay, skip, weight = args
     _, rows, channels = gate_in.shape
-    seq_len, group = (rows * n, channels // n)
+    seq_len = rows * n
+    half = seq_len // 2
     width = weight.shape[1]
-    part = group // PARTS
     slabs = channels // LANES
+    share = (slabs - n) // 2
     table, table_t, turn = wave_tables(seq_len)
+    table_t = table_t[:1]
     features = feature_table(seq_len, first.shape[0])
     vmem = pl.BlockSpec(memory_space=pltpu.VMEM)
     main = pl.BlockSpec(memory_space=pltpu.HBM)
@@ -631,6 +678,7 @@
         in_specs=[main] * 17,
         out_specs=vmem,
         scratch_shapes=[
+            pltpu.VMEM((2, 3, EDGE, channels), bf16),
             pltpu.VMEM((rows, channels), bf16),
             pltpu.VMEM((rows, channels), bf16),
             pltpu.VMEM((rows, channels), bf16),
@@ -641,32 +689,38 @@
             pltpu.VMEM((1, channels), f32),
             pltpu.VMEM((1, channels), f32),
             pltpu.VMEM((FEATS, hidden_count), f32),
-            pltpu.VMEM((hidden_count, group), f32),
-            pltpu.VMEM((hidden_count, group), f32),
+            pltpu.VMEM((hidden_count, (1 + share) * LANES), f32),
+            pltpu.VMEM((hidden_count, (1 + share) * LANES), f32),
             pltpu.VMEM(weight.shape, bf16),
             pltpu.VMEM(table.shape, bf16),
             pltpu.VMEM(table_t.shape, bf16),
             pltpu.VMEM(turn.shape, f32),
             pltpu.VMEM(features.shape, bf16),
-            pltpu.VMEM((PARTS, n, rows + EDGE, part), bf16),
-            pltpu.VMEM((PARTS, n, rows + EDGE, part), bf16),
-            pltpu.VMEM((PARTS, seq_len, 2 * part), bf16),
-            pltpu.VMEM((PARTS, n, rows, part), bf16),
-            pltpu.VMEM((PARTS, n, rows, part), bf16),
             pltpu.VMEM((2, slabs, 3 * LANES), bf16),
             pltpu.VMEM((2, slabs, 3 * LANES), bf16),
-            pltpu.VMEM((PARTS, seq_len // 2, 2 * part), f32),
-            pltpu.VMEM((PARTS, seq_len // 2, 2 * part), f32),
-            pltpu.VMEM((PARTS, seq_len, 2 * part), bf16),
-            pltpu.VMEM((n, rows, group), f32),
-            pltpu.VMEM((n, rows, group), f32),
+            pltpu.VMEM((n, rows + EDGE, LANES), bf16),
+            pltpu.VMEM((n, rows + EDGE, LANES), bf16),
+            pltpu.VMEM((2 * share, rows, LANES), bf16),
+            pltpu.VMEM((2, 2 * share, EDGE, LANES), bf16),
+            pltpu.VMEM((share, seq_len, LANES), bf16),
+            pltpu.VMEM((n, rows, LANES), bf16),
+            pltpu.VMEM((n, rows, LANES), bf16),
+            pltpu.VMEM((share, rows, LANES), bf16),
+            pltpu.VMEM((share, rows, LANES), bf16),
+            pltpu.VMEM((1 + share, half, 2 * LANES), f32),
+            pltpu.VMEM((1 + share, half, 2 * LANES), f32),
+            pltpu.VMEM((1 + share, seq_len, 2 * LANES), bf16),
+            pltpu.VMEM((slabs, rows, LANES), f32),
+            pltpu.VMEM((slabs, rows, LANES), f32),
             pltpu.VMEM((rows, width), f32),
-            dma((15,)),
-            dma((2, n)),
-            dma((PARTS, n)),
-            dma((PARTS, n)),
-            dma((PARTS, n)),
-            dma((PARTS, n)),
+            dma((32,)),
+            dma((n,)),
+            dma((n,)),
+            dma((3, n)),
+            dma((3, n)),
+            dma((n,)),
+            dma((n,)),
+            dma((2,)),
             dma((2,)),
             dma((2,)),
         ],
@@ -682,9 +736,10 @@
 
 def body_for(n, *args):
     _, rows, channels = args[0].shape
-    small = rows * n <= 1024 and rows % 128 == 0 and channels % (128 * PARTS * n) == 0
+    small = rows * n <= 1024 and rows % 128 == 0 and channels % (2 * LANES) == 0
+    spare = channels // LANES > n
     network = args[6].shape[0] <= FEATS and args[6].shape[1] == 128
-    if n >= 2 and n % 2 == 0 and small and network and args[3].shape[0] == 3:
+    if n >= 2 and n % 2 == 0 and small and spare and network and args[3].shape[0] == 3:
         return fused_body(n, *args)
     return spread_body(*args)
 

time: 14.5 us -> 13 us (0.90)
  Pallas kernels: 13.5 us -> 12.1 us
    pallas_call x1, Pallas kernels: 13.5 us -> 12.1 us  [fused_body(): pl.pallas_call(functools.partial(conv_kernel, n), out_shape=pltpu.VMEM((1...]
where the time goes in v2:
time: 13 us; the launch traced here: 12.9 us
  Pallas kernels  12.1 us (93%)
  local copies, waits for them, and re-layouts  0.8 us (6%)
    pallas_call x1, Pallas kernels, fused_body(): pl.pallas_call(functools.partial(conv_kernel, n), out_shape=pltpu.VMEM((1...  12.1 us
    unnamed x1, local copies, waits for them, and re-layouts  0.8 us

profile of v2, /device:TPU:0, one launch (start us, length us, event | category | flops | bytes accessed | tf_op | source)
XLA Modules:
  0.0 12.9 jit_solution(2620145187069124300)
XLA Ops:
  0.0 12.1 %shard_map.163 = bf16[1,128,2048]{2,1,0:T(8,128)(2,1)S(1)} custom-call(bf16[1,128,1024]{2,1,0:T(8,128)(2,1)} %gate_hbm.1, bf16[1,128,1024]{2,1,0:T(8,128)(2,1)} %mult_hbm.1, bf16[1,128,1024]{2,1,0:T(8,128)(2,1)} %value_hbm.1, f32[3,1024]{1,0:T(4,128)} %taps_gate_hbm.1, f32[3,1024]{1,0:T(4,128)} %taps_mult_hbm.1, f32[3,1024]{1,0:T(4,128)} %taps_value_hbm.1, ...), custom_call_target="tpu_custom_call" | custom-call | tf_op jit(solution)/shard_map/pallas_call | solution.py:675
  12.1 0.8 %copy.19 = bf16[1,128,2048]{2,1,0:T(8,128)(2,1)} copy(bf16[1,128,2048]{2,1,0:T(8,128)(2,1)S(1)} %shard_map.163) | data formatting | bytes 1048576

commit v3 on v2

--- a/solution.py
+++ b/solution.py
@@ -184,6 +184,7 @@
 
 f32, bf16 = (jnp.float32, jnp.bfloat16)
 EDGE = 16
+ENDS = 8
 LANES = 128
 FEATS = 64
 
@@ -314,6 +315,7 @@
     gate_part,
     direct,
     total,
+    partial,
     load_sems,
     send_sems,
     recv_sems,
@@ -321,7 +323,8 @@
     wide_recv,
     back_send,
     back_recv,
-    near_sems,
+    near_send,
+    near_recv,
     halo_send,
     halo_recv,
 ):
@@ -339,6 +342,7 @@
         far += [chip, chip + 1]
     peers = far + [near]
 
+    halo_came[...] = jnp.zeros_like(halo_came)
     barrier = pltpu.get_barrier_semaphore()
     for peer in peers:
         pl.semaphore_signal(
@@ -410,10 +414,19 @@
             )
         halo_sent[side] = jnp.concatenate(parts, axis=1).astype(bf16)
     pl.semaphore_wait(barrier, n - 1)
-    for side, target in enumerate((right, left)):
-        send(
-            halo_sent.at[side], halo_came.at[side], halo_send.at[side], halo_recv.at[side], target
+
+    def halo(side):
+        return remote(
+            halo_sent.at[side],
+            halo_came.at[side],
+            halo_send.at[side],
+            halo_recv.at[side],
+            (right, left)[side],
         )
+
+    inside = (me < n - 1, me > 0)
+    for side in range(2):
+        pl.when(inside[side])(halo(side).start)
 
     zero = jnp.zeros((1, LANES), f32)
 
@@ -426,8 +439,8 @@
         v = value[:, lanes(owner)].astype(f32)
         m = mult[:, lanes(owner)].astype(f32)
         sent[owner, pl.ds(0, rows), :] = short_product(v, m, owner)
-        edges = [v[0:2], v[rows - 2 : rows], m[0:2], m[rows - 2 : rows], jnp.zeros((8, LANES), f32)]
-        sent[owner, pl.ds(rows, EDGE), :] = jnp.concatenate(edges, axis=0).astype(bf16)
+        edges = [v[0:2], v[rows - 2 : rows], m[0:2], m[rows - 2 : rows]]
+        sent[owner, pl.ds(rows, ENDS), :] = jnp.concatenate(edges, axis=0).astype(bf16)
 
     ready("taps_value", "taps_mult", "value0", "mult0")
     for peer in peers:
@@ -503,7 +516,7 @@
     ready("table", "turn")
     cos_half = turn[0][:, 0:1]
     sin_half = turn[1][:, 0:1]
-    for j in range(1 + share):
+    def transform(j):
         cols = slice(j * LANES, (j + 1) * LANES)
         sh, sl = split(sums[:, cols])
         gh, gl = split(gaps[:, cols])
@@ -520,12 +533,13 @@
         kernel_re[j] = cos_half * top + sin_half * bottom
         kernel_im[j] = sin_half * top - cos_half * bottom
 
-    for side, target in enumerate((right, left)):
-        remote(
-            halo_sent.at[side], halo_came.at[side], halo_send.at[side], halo_recv.at[side], target
-        ).wait_recv()
-    befores = halo_came[0].astype(f32) * (me > 0).astype(f32)
-    afters = halo_came[1].astype(f32) * (me < n - 1).astype(f32)
+    for j in range(0):
+        transform(j)
+    for side in range(2):
+        pl.when(inside[1 - side])(halo(side).wait_recv)
+        pl.when(inside[side])(halo(side).wait_send)
+    befores = halo_came[0].astype(f32)
+    afters = halo_came[1].astype(f32)
 
     def line_of(halo, i, slab):
         return halo[slab : slab + 1, i * LANES : (i + 1) * LANES]
@@ -562,10 +576,12 @@
         for side in range(2):
             wide_came[j, rim_of(me, side), :] = rim_sent[side, core * share + j]
 
+    for j in range(0, 1 + share):
+        transform(j)
+
     alternate = signs((rows, LANES))
 
-    def convolve(j, x):
-        freq = mul(table[0], jnp.concatenate([x, x * flip], axis=1))
+    def convolve(j, freq):
         top, bottom = (freq[:half], freq[half:])
         kr, ki = (kernel_re[j], kernel_im[j])
         spec[j, :half] = (top * kr + bottom * ki).astype(bf16)
@@ -581,7 +597,7 @@
         remote(
             sent.at[peer], came.at[peer], send_sems.at[peer], recv_sems.at[peer], peer
         ).wait_recv()
-    edges = [came[s, pl.ds(rows, EDGE), :].astype(f32) for s in range(n)]
+    edges = [came[s, pl.ds(rows, ENDS), :].astype(f32) for s in range(n)]
     own_taps = [t[:, lanes(me)] for t in (taps_value, taps_mult)]
     pieces = []
     for s in range(n):
@@ -600,7 +616,8 @@
         lower = jnp.where(rim_at == EDGE - 1, bottom, block[rows - EDGE :].astype(f32)).astype(bf16)
         pieces += [upper, block[EDGE : rows - EDGE], lower]
     ready("table_t")
-    convolve(0, jnp.concatenate(pieces, axis=0))
+    x = jnp.concatenate(pieces, axis=0)
+    convolve(0, mul(table[0], jnp.concatenate([x, x * flip], axis=1)))
     for peer in peers:
         back_sent[peer] = invert(peer, 0).astype(bf16)
         send(back_sent.at[peer], back_came.at[me], back_send.at[peer], back_recv.at[me], peer)
@@ -633,25 +650,36 @@
         ).wait_recv()
         return (peer, back_came[peer].astype(f32))
 
-    for peer in reversed(peers):
+    def gathered(peer):
         for i in range(3):
             where = inner_of(peer) if i == 0 else rim_of(peer, i - 1)
             what = wide_sent.at[own_share(me), inner] if i == 0 else rim_sent.at[i - 1, own_share(me)]
             remote(
                 what, wide_came.at[:, where], wide_send.at[i, peer], wide_recv.at[i, peer], peer
             ).wait_recv()
+
+    def wave(j, chip):
+        where = pl.ds(pl.multiple_of(chip * rows, 2 * rows), 2 * rows)
+        x = wide_came[j, where, :]
+        return mul(table[0, :, where], jnp.concatenate([x, x * flip[: 2 * rows]], axis=1))
+
+    gathered(near)
     for j in range(share):
-        convolve(1 + j, wide_came[j])
+        partial[j] = wave(j, me - core)
+    for peer in reversed(far):
+        gathered(peer)
+    for j in range(share):
+        convolve(1 + j, sum((wave(j, chip) for chip in far[::2]), partial[j]))
     for j in range(share):
         near_sent[j] = invert(near, 1 + j).astype(bf16)
-    send(near_sent, near_came, near_sems.at[0], near_sems.at[1], near)
+    send(near_sent, near_came, near_send.at[0], near_recv.at[0], near)
     items = [(own_wide + j, invert(me, 1 + j)) for j in range(share)]
-    items += [(me, own_back), returned(near)]
-    total[...] = project(items)
+    total[...] = project(items + [(me, own_back), returned(near)])
+    near_wide = n + share * (1 - core)
     items = [returned(peer) for peer in reversed(far)]
-    remote(near_sent, near_came, near_sems.at[0], near_sems.at[1], near).wait_recv()
-    near_wide = n + share * (1 - core)
-    items += [(near_wide + j, near_came[j].astype(f32)) for j in range(share)]
+    remote(near_sent, near_came, near_send.at[0], near_recv.at[0], near).wait_recv()
+    for j in range(share):
+        items.append((near_wide + j, near_came[j].astype(f32)))
     out_ref[0] = (total[...] + project(items)).astype(bf16)
     for copy in copies:
         copy.wait_send()
@@ -698,8 +726,8 @@
             pltpu.VMEM(features.shape, bf16),
             pltpu.VMEM((2, slabs, 3 * LANES), bf16),
             pltpu.VMEM((2, slabs, 3 * LANES), bf16),
-            pltpu.VMEM((n, rows + EDGE, LANES), bf16),
-            pltpu.VMEM((n, rows + EDGE, LANES), bf16),
+            pltpu.VMEM((n, rows + ENDS, LANES), bf16),
+            pltpu.VMEM((n, rows + ENDS, LANES), bf16),
             pltpu.VMEM((2 * share, rows, LANES), bf16),
             pltpu.VMEM((2, 2 * share, EDGE, LANES), bf16),
             pltpu.VMEM((share, seq_len, LANES), bf16),
@@ -713,6 +741,7 @@
             pltpu.VMEM((slabs, rows, LANES), f32),
             pltpu.VMEM((slabs, rows, LANES), f32),
             pltpu.VMEM((rows, width), f32),
+            pltpu.VMEM((share, seq_len, 2 * LANES), f32),
             dma((32,)),
             dma((n,)),
             dma((n,)),
@@ -720,7 +749,8 @@
             dma((3, n)),
             dma((n,)),
             dma((n,)),
-            dma((2,)),
+            dma((share,)),
+            dma((share,)),
             dma((2,)),
             dma((2,)),
         ],

time: 13 us -> 12.6 us (0.969)
  Pallas kernels: 12.1 us -> 11.7 us
    pallas_call x1, Pallas kernels: 12.1 us -> 11.7 us  [fused_body(): pl.pallas_call(functools.partial(conv_kernel, n), out_shape=pltpu.VMEM((1...]
where the time goes in v3:
time: 12.6 us; the launch traced here: 12.5 us
  Pallas kernels  11.7 us (93%)
  local copies, waits for them, and re-layouts  0.8 us (6%)
    pallas_call x1, Pallas kernels, fused_body(): pl.pallas_call(functools.partial(conv_kernel, n), out_shape=pltpu.VMEM((1...  11.7 us
    unnamed x1, local copies, waits for them, and re-layouts  0.8 us

profile of v3, /device:TPU:0, one launch (start us, length us, event | category | flops | bytes accessed | tf_op | source)
XLA Modules:
  0.0 12.5 jit_solution(9626201876347473091)
XLA Ops:
  0.0 11.7 %shard_map.163 = bf16[1,128,2048]{2,1,0:T(8,128)(2,1)S(1)} custom-call(bf16[1,128,1024]{2,1,0:T(8,128)(2,1)} %gate_hbm.1, bf16[1,128,1024]{2,1,0:T(8,128)(2,1)} %mult_hbm.1, bf16[1,128,1024]{2,1,0:T(8,128)(2,1)} %value_hbm.1, f32[3,1024]{1,0:T(4,128)} %taps_gate_hbm.1, f32[3,1024]{1,0:T(4,128)} %taps_mult_hbm.1, f32[3,1024]{1,0:T(4,128)} %taps_value_hbm.1, ...), custom_call_target="tpu_custom_call" | custom-call | tf_op jit(solution)/shard_map/pallas_call | solution.py:703
  11.7 0.8 %copy.19 = bf16[1,128,2048]{2,1,0:T(8,128)(2,1)} copy(bf16[1,128,2048]{2,1,0:T(8,128)(2,1)S(1)} %shard_map.163) | data formatting | bytes 1048576

commit v4 on v3

--- a/solution.py
+++ b/solution.py
@@ -342,13 +342,6 @@
         far += [chip, chip + 1]
     peers = far + [near]
 
-    halo_came[...] = jnp.zeros_like(halo_came)
-    barrier = pltpu.get_barrier_semaphore()
-    for peer in peers:
-        pl.semaphore_signal(
-            barrier, inc=1, device_id={"col": peer}, device_id_type=pl.DeviceIdType.MESH
-        )
-
     def lanes(slab, count=1):
         start = slab * LANES
         if not isinstance(slab, int):
@@ -387,6 +380,13 @@
     for i, (low, count) in enumerate(((0, n), (n, slabs - n))):
         load(f"value{i}", value_hbm.at[0, :, lanes(low, count)], value.at[:, lanes(low, count)])
         load(f"mult{i}", mult_hbm.at[0, :, lanes(low, count)], mult.at[:, lanes(low, count)])
+    halo_came[...] = jnp.zeros_like(halo_came)
+    barrier = pltpu.get_barrier_semaphore()
+    for peer in peers:
+        pl.semaphore_signal(
+            barrier, inc=1, device_id={"col": peer}, device_id_type=pl.DeviceIdType.MESH
+        )
+
     own_wide = n + share * core
     load("feature", feature_hbm, feature)
     load("first", first_hbm, first.at[pl.ds(0, first_hbm.shape[0])])
@@ -433,7 +433,9 @@
     def short_product(v, m, slab):
         vs = short_form(v, taps_value[:, lanes(slab)], zero, zero)
         ms = short_form(m, taps_mult[:, lanes(slab)], zero, zero)
-        return (vs * ms).astype(bf16)
+        product = vs * ms
+        direct[slab] = product
+        return product.astype(bf16)
 
     def pack(owner):
         v = value[:, lanes(owner)].astype(f32)
@@ -497,14 +499,19 @@
     ready("decay", "ahead0", "ahead1", "behind0", "behind1")
     both_rates = [decay_ref[:, lanes(me)], decay_ref[:, lanes(own_wide, share)]]
     rates = jnp.concatenate(both_rates, axis=1) * (-1.0 / (seq_len - 1))
-    index = lax.broadcasted_iota(jnp.int32, (seq_len, (1 + share) * LANES), 0)
-    fade = jnp.exp(rates * index.astype(f32))
+    width = (1 + share) * LANES
+
+    def powers(count, stride):
+        index = lax.broadcasted_iota(jnp.int32, (count, width), 0) * stride
+        return jnp.exp(rates * index.astype(f32))
+
+    coarse, fine = (powers(seq_len // EDGE, EDGE), powers(EDGE, 1))
+    fade = jnp.concatenate([coarse[i : i + 1] * fine for i in range(seq_len // EDGE)], axis=0)
 
     def side_of(values, w):
-        high, low = split(w)
-        return mul(values, jnp.concatenate([high, high], axis=0)) + mul(
-            values, jnp.concatenate([low, low], axis=0)
-        )
+        both = joined(w, 1)
+        wide = mul(values, jnp.concatenate([both, both], axis=0))
+        return wide[:, : w.shape[1]] + wide[:, w.shape[1] :]
 
     ahead = side_of(joined(hidden, 1), ahead_w[...])
     behind = side_of(joined(later, 1), behind_w[...] * jnp.exp(rates))
@@ -545,7 +552,7 @@
         return halo[slab : slab + 1, i * LANES : (i + 1) * LANES]
 
     rim_at = lax.broadcasted_iota(jnp.int32, (EDGE, LANES), 0)
-    for slab in range(n, slabs):
+    def mend(slab):
         first_row = last_row = 1.0
         for i, taps in ((1, taps_mult), (2, taps_value)):
             t = taps[:, lanes(slab)]
@@ -561,8 +568,13 @@
             )
         for side, row, where in ((1, first_row, 0), (0, last_row, EDGE - 1)):
             base = 0 if side else rows - EDGE
-            old = wide_sent[slab - n, base : base + EDGE, :].astype(f32)
-            rim_sent[side, slab - n] = jnp.where(rim_at == where, row, old).astype(bf16)
+            tile = jnp.where(rim_at == where, row, direct[slab, base : base + EDGE, :])
+            direct[slab, base : base + EDGE, :] = tile
+            if slab >= n:
+                rim_sent[side, slab - n] = tile.astype(bf16)
+
+    for slab in range(n, slabs):
+        mend(slab)
     for peer in peers:
         for side in range(2):
             send(
@@ -626,19 +638,15 @@
     ready("gate", "taps_gate", "skip")
     for slab in range(slabs):
         cols = lanes(slab)
-        parts = []
-        for i, (r, taps) in enumerate(((gate, taps_gate), (mult, taps_mult), (value, taps_value))):
-            parts.append(
-                short_form(
-                    r[:, cols].astype(f32), taps[:, cols], line_of(befores, i, slab), line_of(afters, i, slab)
-                )
-            )
-        gate_part[slab] = parts[0]
-        direct[slab] = skip_ref[:, cols] * (parts[1] * parts[2])
+        gate_part[slab] = short_form(
+            gate[:, cols].astype(f32), taps_gate[:, cols], line_of(befores, 0, slab), line_of(afters, 0, slab)
+        )
+    for slab in range(n):
+        mend(slab)
     ready("weight")
 
     def gated(slab, convolved):
-        return ((convolved + direct[slab]) * gate_part[slab]).astype(bf16)
+        return ((convolved + skip_ref[:, lanes(slab)] * direct[slab]) * gate_part[slab]).astype(bf16)
 
     def project(items):
         left_side = jnp.concatenate([gated(slab, value) for slab, value in items], axis=1)

time: 12.6 us -> 12.6 us (level)
  no operation moved by 1% of the time
where the time goes in v4:
time: 12.6 us; the launch traced here: 12.5 us
  Pallas kernels  11.7 us (93%)
  local copies, waits for them, and re-layouts  0.8 us (6%)
    pallas_call x1, Pallas kernels, fused_body(): pl.pallas_call(functools.partial(conv_kernel, n), out_shape=pltpu.VMEM((1...  11.7 us
    unnamed x1, local copies, waits for them, and re-layouts  0.8 us

profile of v4, /device:TPU:0, one launch (start us, length us, event | category | flops | bytes accessed | tf_op | source)
XLA Modules:
  0.0 12.5 jit_solution(9803022825562232442)
XLA Ops:
  0.0 11.7 %shard_map.163 = bf16[1,128,2048]{2,1,0:T(8,128)(2,1)S(1)} custom-call(bf16[1,128,1024]{2,1,0:T(8,128)(2,1)} %gate_hbm.1, bf16[1,128,1024]{2,1,0:T(8,128)(2,1)} %mult_hbm.1, bf16[1,128,1024]{2,1,0:T(8,128)(2,1)} %value_hbm.1, f32[3,1024]{1,0:T(4,128)} %taps_gate_hbm.1, f32[3,1024]{1,0:T(4,128)} %taps_mult_hbm.1, f32[3,1024]{1,0:T(4,128)} %taps_value_hbm.1, ...), custom_call_target="tpu_custom_call" | custom-call | tf_op jit(solution)/shard_map/pallas_call | solution.py:711
  11.7 0.8 %copy.19 = bf16[1,128,2048]{2,1,0:T(8,128)(2,1)} copy(bf16[1,128,2048]{2,1,0:T(8,128)(2,1)S(1)} %shard_map.163) | data formatting | bytes 1048576
